TPU v7x, 128 devices: a whole 4x4x4 slice. The times are simulated.
128 devices in a mesh: sp: 16 (over z, y), dp: 8 (over x, core).
Axes of the slice: x: 4, y: 4, z: 4, core: 2. Of those that a mesh axis runs over, the one named last changes fastest.
Arguments:
- stream: bfloat16 [8, 2048, 2048], P('dp', 'sp'), may hold values from -6 to 6
- queries: bfloat16 [8, 2048, 1024], P('dp', 'sp'), may hold values from -6 to 6
- keys_in: bfloat16 [8, 2048, 1024], P('dp', 'sp'), may hold values from -6 to 6
- values_in: bfloat16 [8, 2048, 1024], P('dp', 'sp'), may hold values from -6 to 6
- key_shift: bfloat16 [8, 2048, 16], P('dp', 'sp'), may hold values from -8 to 16
- head_shift: float32 [16], replicated, may hold values from -16 to 0
- mix_gain: float32 [1024], replicated, may hold values from 0.1 to 1.9
- out_weight: bfloat16 [1024, 2048], replicated, may hold values from -0.1875 to 0.1875
- post_gain: float32 [2048], replicated, may hold values from 0.1 to 1.9
- route: int32 [8, 2048, 2], P('dp', 'sp'), may hold values from 0 to 127, as said below
- route_weight: float32 [8, 2048, 2], P('dp', 'sp'), may hold values from 0.25 to 1
- w_gate: bfloat16 [128, 2048, 1024], P(('sp', 'dp')), may hold values from -0.125 to 0.125
- w_up: bfloat16 [128, 2048, 1024], P(('sp', 'dp')), may hold values from -0.125 to 0.125
- w_down: bfloat16 [128, 1024, 2048], P(('sp', 'dp')), may hold values from -0.1875 to 0.1875
Outputs:
- result: bfloat16 [8, 2048, 2048], P('dp', 'sp')
Inputs may be any that keep to these rules, and one draw needn't show every extreme that they name: `route`: each token names two different experts of one group (the group of expert e is e // 32). Of the 128 tokens of one device, each expert is named by at most 4; in every draw the 32 experts of one group are each named by exactly 4 tokens of every device.
All inputs are finite; a program needn't handle non-finite values.
Results may differ from a plain program's by a relative error of at most 0.0085.
Values may be sent and summed in bfloat16 or wider, within the bound.
A program may use at most 128 MiB of HBM per device.

v0:
```python
import math

import jax
import jax.numpy as jnp
from jax import lax
from jax.sharding import Mesh
from jax.sharding import PartitionSpec as P

HD = 64
GROUPS = 4
EXP_DEV = 1
SP = ("sp_0", "sp_1")
SP_DP = ("sp_0", "sp_1", "dp")


norm_eps = 1e-05


def sent_together(arrays, axis, split_dim, concat_dim, along):
    both = jnp.concatenate(arrays, axis=along)
    result, at, gathered = (
        lax.all_to_all(both, axis, split_axis=split_dim, concat_axis=concat_dim, tiled=True),
        0,
        [],
    )
    for a in arrays:
        gathered.append(lax.slice_in_dim(result, at, at + a.shape[along], axis=along))
        at += a.shape[along]
    return tuple(gathered)


def split_up(x, dim, length):
    lengths = x.shape
    pieces = x.reshape(*lengths[:dim], length, lengths[dim] // length, *lengths[dim + 1 :])
    return jnp.moveaxis(pieces, dim, 0)


def in_order(pieces, dim):
    lengths = list(pieces.shape[1:])
    lengths[dim] *= pieces.shape[0]
    return jnp.moveaxis(pieces, 0, dim).reshape(lengths)


def moved_by_axis(pieces, axes, turns):
    inside = pieces.shape[1:]
    result = pieces.reshape(*(lax.axis_size(a) for a in axes), *inside)
    for k in turns:
        result = lax.all_to_all(result, axes[k], k, k, tiled=True)
    return result.reshape(-1, *inside)


def stepwise_exchange(x, axes, turns, split_dim, concat_dim):
    pieces = split_up(x, split_dim, lax.axis_size(axes))
    return in_order(moved_by_axis(pieces, axes, turns), concat_dim)


def joined_exchange(x, axis, axes, splits, concats):
    sizes = [lax.axis_size(a) for a in axes]
    pieces = split_up(x, splits[0], sizes[0])
    pieces = jnp.moveaxis(split_up(pieces, splits[1] + 1, sizes[1]), 0, 1)
    inside = pieces.shape[2:]
    pieces = pieces.reshape(-1, *inside)
    pieces = lax.all_to_all(pieces, axis, split_axis=0, concat_axis=0, tiled=True)
    pieces = in_order(pieces.reshape(*sizes, *inside), concats[0] + 1)
    return in_order(pieces, concats[1])


def block_total(length):
    blocks = 1
    while blocks * 2 <= min(8, length // 512):
        blocks = blocks * 2
    return blocks


def stick_head(queries_head, keys_head, values_head, offsets):
    length = queries_head.shape[0]
    blocks = block_total(length)
    width = length // blocks
    scale = 1.0 / math.sqrt(HD)
    pieces = []
    for block_idx in range(blocks):
        begin = block_idx * width
        finish = begin + width
        logits = (
            jnp.einsum(
                "qd,kd->qk",
                queries_head[begin:finish],
                keys_head[:finish],
                preferred_element_type=jnp.float32,
            )
            * scale
        )
        logits = logits + offsets[None, :finish]
        rows_pos = begin + jnp.arange(width, dtype=jnp.int32)
        cols_pos = jnp.arange(finish, dtype=jnp.int32)
        causal = cols_pos[None, :] < rows_pos[:, None]
        breaks = jnp.where(causal, jax.nn.log_sigmoid(-logits), 0.0)
        suffix = lax.cumsum(breaks, axis=1, reverse=True) - breaks
        weights = jnp.where(causal, jnp.exp(jax.nn.log_sigmoid(logits) + suffix), 0.0).astype(
            jnp.bfloat16
        )
        pieces.append(jnp.dot(weights, values_head[:finish], preferred_element_type=jnp.float32))
    return jnp.concatenate(pieces, axis=0).astype(jnp.bfloat16)


def on_device(
    stream,
    queries,
    keys_in,
    values_in,
    key_shift,
    head_shift,
    mix_gain,
    out_weight,
    post_gain,
    route,
    route_weight,
    w_gate,
    w_up,
    w_down,
):
    tokens = stream.shape[1]
    width = stream.shape[2]
    head_q, head_k, head_v, head_off = (
        *sent_together((queries, keys_in, values_in), SP, 2, 1, 0),
        lax.all_to_all(key_shift, SP, split_axis=2, concat_axis=1, tiled=True),
    )
    local_heads = head_off.shape[2]
    first_head = lax.axis_index(SP) * local_heads
    own_shift = lax.dynamic_slice_in_dim(head_shift, first_head, local_heads)
    cols = slice(0, HD)
    offsets = head_off[0, :, 0].astype(jnp.float32) + own_shift[0]
    outputs = stick_head(head_q[0, :, cols], head_k[0, :, cols], head_v[0, :, cols], offsets)
    attended_heads = outputs[None]
    attended = stepwise_exchange(attended_heads, SP, (0, 1), 1, 2)[0]
    att32 = attended.astype(jnp.float32)
    normed = (
        att32 * lax.rsqrt(jnp.mean(att32 * att32, axis=1, keepdims=True) + norm_eps) * mix_gain
    ).astype(jnp.bfloat16)
    mixed = jnp.dot(normed, out_weight, preferred_element_type=jnp.float32)
    summed = stream[0].astype(jnp.float32) + mixed
    hidden = (
        summed * lax.rsqrt(jnp.mean(summed * summed, axis=1, keepdims=True) + norm_eps) * post_gain
    ).astype(jnp.bfloat16)
    size_sp = lax.axis_size(SP)
    size_dp = lax.axis_size("dp")
    n_expert = EXP_DEV * size_sp * size_dp
    per_group = n_expert // GROUPS
    capacity = tokens // per_group
    expert_ids = route[0].reshape(tokens * 2)
    onehot = (expert_ids[:, None] == jnp.arange(n_expert, dtype=jnp.int32)[None, :]).astype(
        jnp.int32
    )
    ranks = jnp.sum((jnp.cumsum(onehot, axis=0) - onehot) * onehot, axis=1)
    dest = expert_ids * capacity + ranks
    rows = jnp.repeat(hidden, 2, axis=0)
    buffer = jnp.zeros((n_expert * capacity, width), jnp.bfloat16).at[dest].set(rows)
    sendable = buffer.reshape(size_sp, size_dp, EXP_DEV * capacity, width)
    received = joined_exchange(sendable, SP_DP, (SP, "dp"), (0, 1), (0, 1))
    expert_received = received.reshape(size_sp * size_dp, EXP_DEV, capacity, width)
    gate = jnp.einsum("sxcd,xdf->sxcf", expert_received, w_gate, preferred_element_type=jnp.float32)
    upper = jnp.einsum("sxcd,xdf->sxcf", expert_received, w_up, preferred_element_type=jnp.float32)
    inner = (jax.nn.silu(gate) * upper).astype(jnp.bfloat16)
    reply_result = jnp.einsum(
        "sxcf,xfd->sxcd", inner, w_down, preferred_element_type=jnp.float32
    ).astype(jnp.bfloat16)
    reply_result = reply_result.reshape(size_sp, size_dp, EXP_DEV * capacity, width)
    returned = joined_exchange(reply_result, SP_DP, (SP, "dp"), (0, 1), (0, 1))
    returned = returned.reshape(n_expert * capacity, width)
    picked = returned[dest].astype(jnp.float32).reshape(tokens, 2, width)
    moe_sum = jnp.sum(picked * route_weight[0][:, :, None], axis=1)
    result = (hidden.astype(jnp.float32) + moe_sum).astype(jnp.bfloat16)
    return result[None]


def solution(mesh):
    finer = Mesh(mesh.devices.reshape(4, 4, mesh.shape["dp"]), ("sp_0", "sp_1", "dp"))
    placed = (
        P("dp", SP, None),
        P("dp", SP, None),
        P("dp", SP, None),
        P("dp", SP, None),
        P("dp", SP, None),
        P(),
        P(),
        P(),
        P(),
        P("dp", SP, None),
        P("dp", SP, None),
        P(SP_DP, None, None),
        P(SP_DP, None, None),
        P(SP_DP, None, None),
    )
    return jax.shard_map(
        on_device, mesh=finer, in_specs=placed, out_specs=P("dp", SP, None), check_vma=False
    )
```

profile of v0, /device:TPU:1, one launch (start us, length us, event | category | flops | bytes accessed | tf_op | source)
XLA Modules:
  0.0 295.8 jit_solution(6585007960604439033)
XLA Ops:
  1.3 8.6 %all-to-all-start.1 = ((bf16[1,128,16]{1,0,2:T(2,128)(2,1)}), bf16[1,128,16]{1,0,2:T(2,128)(2,1)S(1)}, u32[]{:S(2)}, u32[]{:S(2)}) async-start(bf16[1,128,16]{1,0,2:T(2,128)(2,1)} %copy.65), calls=%async_computation.1 | async-start | bytes 16384 | tf_op jit(solution)/shard_map/all_to_all | solution.py:126
  15.7 2.8 pad_maximum_fusion
  19.7 6.9 %all-to-all-start = ((bf16[3,128,1024]{1,0,2:T(4,128)(2,1)}), bf16[3,128,1024]{1,0,2:T(4,128)(2,1)S(1)}, u32[]{:S(2)}, u32[]{:S(2)}) async-start(bf16[3,128,1024]{1,0,2:T(4,128)(2,1)} %pad_maximum_fusion), calls=%async_computation | async-start | bytes 2097152 | tf_op jit(solution)/shard_map/all_to_all | solution.py:22
  27.3 14.8 %all-to-all-done = bf16[3,128,1024]{1,0,2:T(4,128)(2,1)S(1)} async-done(((bf16[3,128,1024]{1,0,2:T(4,128)(2,1)}), bf16[3,128,1024]{1,0,2:T(4,128)(2,1)S(1)}, u32[]{:S(2)}, u32[]{:S(2)}) %all-to-all-start) | async-done | bytes 786464 | tf_op jit(solution)/shard_map/all_to_all | solution.py:22
  43.9 1.7 fusion.76
  45.5 4.8 %fusion.77 = f32[512,4,128]{0,1,2:T(4,128)S(1)} fusion(f32[512,4,128]{0,2,1:T(8,128)S(1)} %bitcast.295), kind=kOutput, calls=%fused_computation.85 | output fusion | flops 33292288 | bytes 2097152 | tf_op jit(solution)/shard_map/reduce-window
  53.1 1.5 fusion.49
  55.1 2.6 copy.71
  57.7 5.9 %fusion.128 = f32[512,8,128]{0,1,2:T(8,128)S(1)} fusion(f32[512,8,128]{0,1,2:T(8,128)} %copy.71), kind=kOutput, calls=%fused_computation.164 | output fusion | flops 66584576 | bytes 4194304 | tf_op jit(solution)/shard_map/reduce-window.2
  63.7 1.6 broadcast_add_fusion.2
  65.3 3.1 %copy.72 = f32[512,8,128]{2,1,0:T(8,128)} copy(f32[512,8,128]{0,1,2:T(8,128)} %broadcast_add_fusion.2) | data formatting | bytes 4194304 | tf_op jit(solution)/shard_map/reduce_window_sum | solution.py:98
  69.3 5.1 %fusion.22 = (f32[512,1536]{1,0:T(8,128)}, f32[512,1536]{1,0:T(8,128)}) fusion(s32[512]{0:T(512)S(1)} %iota_add_fusion.1, f32[1536]{0:T(1024)S(1)} %slice_bitcast_fusion.3, bf16[8,8,12,128]{3,2,1,0:T(8,128)(2,1)S(1)} %bitcast.301, bf16[8,8,4,128]{3,2,1,0:T(4,128)(2,1)S(1)} %bitcast.313), kind=kOutput, calls=%fused_computation.34 | convolution fusion | flops 109314048 | bytes 6561792 | tf_op jit(solution)/shard_map/qd,kd->qk/dot_general | solution.py:85
  74.5 2.4 copy.76
  76.9 10.3 %fusion.13 = f32[512,12,128]{0,1,2:T(8,128)S(1)} fusion(f32[512,12,128]{0,2,1:T(8,128)S(1)} %bitcast.279), kind=kOutput, calls=%fused_computation.22 | output fusion | flops 99876864 | bytes 6291456 | tf_op jit(solution)/shard_map/reduce-window.4
  87.1 1.9 copy-done.1
  89.2 2.7 broadcast_add_fusion.1
  91.9 1.8 copy.78
  93.7 2.4 copy.79
  96.1 1.8 copy.80
  99.8 2.9 fusion.23
  102.8 2.9 copy.111
  105.6 5.8 %copy.83 = f32[512,16,128]{0,1,2:T(8,128)} copy(f32[512,16,128]{2,1,0:T(8,128)} %bitcast.278) | data formatting | bytes 8388608 | tf_op jit(solution)/shard_map/reshape.16
  111.4 10.8 %fusion.129 = f32[512,16,128]{0,1,2:T(8,128)S(1)} fusion(f32[512,16,128]{0,1,2:T(8,128)} %copy.83), kind=kOutput, calls=%fused_computation.165 | output fusion | flops 133169152 | bytes 8388608 | tf_op jit(solution)/shard_map/reduce-window.6
  122.2 2.0 copy-done
  124.3 5.1 %broadcast_add_fusion = f32[512,16,128]{0,1,2:T(8,128)} fusion(f32[512,16,128]{0,1,2:T(8,128)} %copy-done, f32[512,16]{0,1:T(8,128)S(1)} %slice.189), kind=kLoop, calls=%fused_computation.60 | loop fusion | flops 1048576 | bytes 8421376 | tf_op jit(solution)/shard_map/reduce_window_sum | solution.py:98
  129.4 6.4 %copy.84 = f32[512,16,128]{2,1,0:T(8,128)} copy(f32[512,16,128]{0,1,2:T(8,128)} %broadcast_add_fusion) | data formatting | bytes 8388608 | tf_op jit(solution)/shard_map/reduce_window_sum | solution.py:98
  136.0 2.3 fusion.74
  138.6 3.2 %convolution_convert_fusion = bf16[512,64]{0,1:T(8,128)(2,1)S(1)} fusion(f32[64,8,8,128]{3,2,1,0:T(8,128)S(1)} %bitcast.291, f32[512,1024]{1,0:T(8,128)S(1)} %copy-done.5, f32[1024]{0:T(1024)S(1)} %slice_bitcast_fusion.5, s32[512]{0:T(512)S(1)} %iota_add_fusion.2, bf16[8,8,8,128]{3,2,1,0:T(8,128)(2,1)S(1)} %bitcast.305), kind=kOutput, calls=%fused_computation.72 | convolution fusion | flops 79200256 | bytes 4397056 | tf_op jit(solution)/shard_map/dot_general | solution.py:102
  142.1 7.1 %fusion.63 = bf16[512,64]{0,1:T(8,128)(2,1)S(1)} fusion(f32[64,8,16,128]{3,2,1,0:T(8,128)S(1)} %bitcast.289, f32[512,2048]{1,0:T(8,128)S(1)} %copy-done.3, f32[2048]{0:T(1024)S(1)} %bitcast.310, s32[512]{0:T(512)S(1)} %copy-done.18, bf16[8,8,16,128]{3,2,1,0:T(8,128)(2,1)S(1)} %bitcast.304), kind=kOutput, calls=%fused_computation.74 | convolution fusion | flops 158367744 | bytes 8726528 | tf_op jit(solution)/shard_map/dot_general | solution.py:102
  149.3 4.6 %fusion.60 = bf16[512,64]{0,1:T(8,128)(2,1)S(1)} fusion(f32[512,1536]{1,0:T(8,128)S(1)} %copy-done.9, f32[512,1536]{1,0:T(8,128)S(1)} %copy-done.26, s32[512]{0:T(512)S(1)} %copy-done.22, bf16[8,8,12,128]{3,2,1,0:T(8,128)(2,1)S(1)} %bitcast.300), kind=kOutput, calls=%fused_computation.73 | convolution fusion | flops 117211136 | bytes 6555648 | tf_op jit(solution)/shard_map/dot_general | solution.py:102
  154.9 3.4 %all-to-all-start.2 = ((bf16[4,4,1,128,64]{3,1,4,2,0:T(4,128)(2,1)}), bf16[4,4,1,128,64]{3,1,4,2,0:T(4,128)(2,1)S(1)}, u32[]{:S(2)}, u32[]{:S(2)}) async-start(bf16[4,4,1,128,64]{3,1,4,2,0:T(4,128)(2,1)} %copy.86), calls=%async_computation.2 | async-start | bytes 524288 | tf_op jit(solution)/shard_map/all_to_all | solution.py:48
  158.9 4.9 %all-to-all-done.2 = bf16[4,4,1,128,64]{3,1,4,2,0:T(4,128)(2,1)S(1)} async-done(((bf16[4,4,1,128,64]{3,1,4,2,0:T(4,128)(2,1)}), bf16[4,4,1,128,64]{3,1,4,2,0:T(4,128)(2,1)S(1)}, u32[]{:S(2)}, u32[]{:S(2)}) %all-to-all-start.2) | async-done | bytes 262176 | tf_op jit(solution)/shard_map/all_to_all | solution.py:48
  164.7 3.5 %all-to-all-start.3 = ((bf16[4,4,1,128,64]{3,0,4,2,1:T(4,128)(2,1)}), bf16[4,4,1,128,64]{3,0,4,2,1:T(4,128)(2,1)S(1)}, u32[]{:S(2)}, u32[]{:S(2)}) async-start(bf16[4,4,1,128,64]{3,0,4,2,1:T(4,128)(2,1)} %copy.87), calls=%async_computation.3 | async-start | bytes 524288 | tf_op jit(solution)/shard_map/all_to_all | solution.py:48
  168.2 5.5 %all-to-all-done.3 = bf16[4,4,1,128,64]{3,0,4,2,1:T(4,128)(2,1)S(1)} async-done(((bf16[4,4,1,128,64]{3,0,4,2,1:T(4,128)(2,1)}), bf16[4,4,1,128,64]{3,0,4,2,1:T(4,128)(2,1)S(1)}, u32[]{:S(2)}, u32[]{:S(2)}) %all-to-all-start.3) | async-done | bytes 262176 | tf_op jit(solution)/shard_map/all_to_all | solution.py:48
  174.3 3.0 %multiply_reduce_fusion.1 = (f32[128]{0:T(128)S(1)}, f32[128,2048]{1,0:T(8,128)S(1)}) fusion(bf16[128,1024]{0,1:T(8,128)(2,1)S(1)} %fusion.85, bf16[1024,2048]{1,0:T(8,128)(2,1)} %param.21, bf16[1,128,2048]{2,1,0:T(8,128)(2,1)S(1)} %copy-done.11), kind=kOutput, calls=%fused_computation.92 | convolution fusion | flops 537919360 | bytes 6029824 | tf_op jit(solution)/shard_map/dot_general | solution.py:140
  179.4 3.5 %scatter_custom_fusion = bf16[512,2048]{1,0:T(8,128)(2,1)S(1)} fusion(s32[256]{0:T(256)S(1)} %bitcast.317, bf16[256,2048]{1,0:T(8,128)(2,1)} %reshape.247, bf16[]{:T(256)} %constant.70.clone.1), kind=kCustom, calls=%fused_computation.89 | custom fusion | bytes 2097664 | tf_op jit(solution)/shard_map/scatter | solution.py:157
  182.9 2.2 reshape_transpose_transpose_reshape_reshape_reshape.6
  185.1 41.0 %all_to_all.44 = bf16[128,1,1,4,2048]{4,3,2,1,0:T(4,128)(2,1)S(1)} all-to-all(bf16[128,1,1,4,2048]{4,3,2,1,0:T(4,128)(2,1)} %bitcast.283), channel_id=1, replica_groups=mesh['sp_0'=4,'sp_1'=4,'dp'=8] {'sp_0','sp_1','dp'}, dimensions={0} | all-to-all | bytes 4194304 | tf_op jit(solution)/shard_map/all_to_all | solution.py:63
  226.1 5.2 %fusion.9 = f32[128,4,1024]{2,0,1:T(8,128)} fusion(bf16[1,2048,1024]{2,1,0:T(8,128)(2,1)S(1)} %copy-done.24, bf16[16,8,1,1,4,2048]{5,4,1,0,3,2:T(4,128)(2,1)S(1)} %bitcast.292), kind=kOutput, calls=%fused_computation.18 | convolution fusion | flops 2147483648 | bytes 8388608 | tf_op jit(solution)/shard_map/sxcd,xdf->sxcf/dot_general | solution.py:162
  231.3 11.5 %fusion.27 = bf16[128,1,1,4,2048]{4,0,3,2,1:T(8,128)(2,1)} fusion(bf16[1,1024,2048]{2,1,0:T(8,128)(2,1)} %param.27, f32[128,4,1024]{2,0,1:T(8,128)} %fusion.9, bf16[1,2048,1024]{2,1,0:T(8,128)(2,1)} %param.25, bf16[16,8,1,1,4,2048]{5,4,1,0,3,2:T(4,128)(2,1)S(1)} %bitcast.293), kind=kOutput, calls=%fused_computation.40 | convolution fusion | flops 4299161600 | bytes 14680064 | tf_op jit(solution)/shard_map/sxcf,xfd->sxcd/dot_general | solution.py:164
  242.9 4.5 %copy.96 = bf16[128,1,1,4,2048]{4,3,2,1,0:T(4,128)(2,1)} copy(bf16[128,1,1,4,2048]{4,0,3,2,1:T(8,128)(2,1)} %fusion.27) | data formatting | bytes 4194304 | tf_op jit(solution)/shard_map/reshape;transpose;transpose;reshape;reshape;reshape | solution.py:62
  247.4 4.9 %all-to-all-start.5 = ((bf16[128,1,1,4,2048]{4,3,2,1,0:T(4,128)(2,1)}), bf16[128,1,1,4,2048]{4,3,2,1,0:T(4,128)(2,1)S(1)}, u32[]{:S(2)}, u32[]{:S(2)}) async-start(bf16[128,1,1,4,2048]{4,3,2,1,0:T(4,128)(2,1)} %copy.96), calls=%async_computation.5 | async-start | bytes 4194304 | tf_op jit(solution)/shard_map/all_to_all | solution.py:63
  252.4 30.4 %all-to-all-done.5 = bf16[128,1,1,4,2048]{4,3,2,1,0:T(4,128)(2,1)S(1)} async-done(((bf16[128,1,1,4,2048]{4,3,2,1,0:T(4,128)(2,1)}), bf16[128,1,1,4,2048]{4,3,2,1,0:T(4,128)(2,1)S(1)}, u32[]{:S(2)}, u32[]{:S(2)}) %all-to-all-start.5) | async-done | bytes 2097184 | tf_op jit(solution)/shard_map/all_to_all | solution.py:63
  282.8 1.3 copy-done.6
  284.1 2.5 reshape_reshape.4
  286.7 2.3 gather_fusion
  289.0 2.4 reshape.233
  291.4 3.2 %multiply_reduce_fusion = f32[128,2048]{1,0:T(8,128)S(1)} fusion(f32[128,2,2048]{2,1,0:T(2,128)S(1)} %reshape.233, f32[128,2]{1,0:T(8,128)S(1)} %copy.97), kind=kLoop, calls=%fused_computation.59 | loop fusion | flops 786432 | bytes 3146752 | tf_op jit(solution)/shard_map/reduce_sum | solution.py:171
  (130 shorter events, 23.7 us)
Async XLA Ops:
  0.0 19.1 %copy-start.25 = (f32[16]{0:T(128)S(1)}, f32[16]{0:T(128)}, u32[]{:S(2)}) copy-start(f32[16]{0:T(128)} %param.19) | copy-start | bytes 196
  1.3 18.4 %all-to-all-start.1 = ((bf16[1,128,16]{1,0,2:T(2,128)(2,1)}), bf16[1,128,16]{1,0,2:T(2,128)(2,1)S(1)}, u32[]{:S(2)}, u32[]{:S(2)}) async-start(bf16[1,128,16]{1,0,2:T(2,128)(2,1)} %copy.65), calls=%async_computation.1 | async-start | bytes 16384 | tf_op jit(solution)/shard_map/all_to_all | solution.py:126
  9.9 59.4 %copy-start.21 = (s32[512]{0:T(512)}, s32[512]{0:T(512)S(1)}, u32[]{:S(2)}) copy-start(s32[512]{0:T(512)S(1)} %iota_add_fusion.1) | copy-start | bytes 6148
  19.7 22.4 %all-to-all-start = ((bf16[3,128,1024]{1,0,2:T(4,128)(2,1)}), bf16[3,128,1024]{1,0,2:T(4,128)(2,1)S(1)}, u32[]{:S(2)}, u32[]{:S(2)}) async-start(bf16[3,128,1024]{1,0,2:T(4,128)(2,1)} %pad_maximum_fusion), calls=%async_computation | async-start | bytes 2097152 | tf_op jit(solution)/shard_map/all_to_all | solution.py:22
  53.1 2.0 copy-start.4
  87.1 1.9 copy-start.1
  96.1 3.7 %copy-start.17 = (s32[512]{0:T(512)S(1)}, s32[512]{0:T(512)}, u32[]{:S(2)}) copy-start(s32[512]{0:T(512)} %iota_add_fusion) | copy-start | bytes 6148
  99.8 3.0 %copy-start.2 = (f32[512,2048]{1,0:T(8,128)}, f32[512,2048]{1,0:T(8,128)S(1)}, u32[]{:S(2)}) copy-start(f32[512,2048]{1,0:T(8,128)S(1)} %fusion.88) | copy-start | bytes 12582916
  122.2 2.0 copy-start
  129.4 6.6 %copy-start.8 = (f32[512,4,128]{0,2,1:T(8,128)S(1)}, f32[512,4,128]{0,2,1:T(8,128)}, u32[]{:S(2)}) copy-start(f32[512,4,128]{0,2,1:T(8,128)} %copy.67) | copy-start | bytes 3145732
  129.4 9.1 %copy-start.10 = (f32[512,8,128]{2,1,0:T(8,128)S(1)}, f32[512,8,128]{2,1,0:T(8,128)}, u32[]{:S(2)}) copy-start(f32[512,8,128]{2,1,0:T(8,128)} %copy.72) | copy-start | bytes 6291460
  135.8 2.5 copy-start.14
  135.8 2.8 copy-start.5
  135.8 2.8 copy-start.15
  138.6 3.3 %copy-start.3 = (f32[512,2048]{1,0:T(8,128)S(1)}, f32[512,2048]{1,0:T(8,128)}, u32[]{:S(2)}) copy-start(f32[512,2048]{1,0:T(8,128)} %copy-done.2) | copy-start | bytes 12582916
  138.6 3.5 %copy-start.7 = (f32[512,16,128]{2,1,0:T(8,128)S(1)}, f32[512,16,128]{2,1,0:T(8,128)}, u32[]{:S(2)}) copy-start(f32[512,16,128]{2,1,0:T(8,128)} %copy.84) | copy-start | bytes 12582916
  138.6 3.5 %copy-start.18 = (s32[512]{0:T(512)S(1)}, s32[512]{0:T(512)}, u32[]{:S(2)}) copy-start(s32[512]{0:T(512)} %iota_add_fusion) | copy-start | bytes 6148
  142.1 7.1 %copy-start.9 = (f32[512,1536]{1,0:T(8,128)S(1)}, f32[512,1536]{1,0:T(8,128)}, u32[]{:S(2)}) copy-start(f32[512,1536]{1,0:T(8,128)} %copy.79) | copy-start | bytes 9437188
  142.1 7.1 %copy-start.13 = (bf16[1,12,128,64]{2,1,3,0:T(8,128)(2,1)S(1)}, bf16[1,12,128,64]{2,1,3,0:T(8,128)(2,1)}, u32[]{:S(2)}) copy-start(bf16[1,12,128,64]{2,1,3,0:T(8,128)(2,1)} %copy.80) | copy-start | bytes 589828
  142.1 7.1 %copy-start.22 = (s32[512]{0:T(512)S(1)}, s32[512]{0:T(512)}, u32[]{:S(2)}) copy-start(s32[512]{0:T(512)} %copy-done.21) | copy-start | bytes 6148
  142.1 7.1 %copy-start.26 = (f32[512,1536]{1,0:T(8,128)S(1)}, f32[512,1536]{1,0:T(8,128)}, u32[]{:S(2)}) copy-start(f32[512,1536]{1,0:T(8,128)} %get-tuple-element.18) | copy-start | bytes 9437188
  149.2 9.1 %copy-start.20 = (s32[1,128,2]{1,2,0:T(2,128)S(1)}, s32[1,128,2]{1,2,0:T(2,128)}, u32[]{:S(2)}) copy-start(s32[1,128,2]{1,2,0:T(2,128)} %param.23) | copy-start | bytes 3076
  149.2 9.2 %copy-start.12 = (s32[128,8,32]{0,1,2:T(8,128)S(1)}, s32[128,8,32]{0,1,2:T(8,128)}, u32[]{:S(2)}) copy-start(s32[128,8,32]{0,1,2:T(8,128)} %broadcast_add_fusion.4) | copy-start | bytes 393220
  153.9 20.2 %copy-start.19 = (f32[1024]{0:T(1024)S(1)}, f32[1024]{0:T(1024)}, u32[]{:S(2)}) copy-start(f32[1024]{0:T(1024)} %param.20) | copy-start | bytes 12292
  153.9 20.4 %copy-start.11 = (bf16[1,128,2048]{2,1,0:T(8,128)(2,1)S(1)}, bf16[1,128,2048]{2,1,0:T(8,128)(2,1)}, u32[]{:S(2)}) copy-start(bf16[1,128,2048]{2,1,0:T(8,128)(2,1)} %param.14) | copy-start | bytes 1572868
  154.9 8.9 %all-to-all-start.2 = ((bf16[4,4,1,128,64]{3,1,4,2,0:T(4,128)(2,1)}), bf16[4,4,1,128,64]{3,1,4,2,0:T(4,128)(2,1)S(1)}, u32[]{:S(2)}, u32[]{:S(2)}) async-start(bf16[4,4,1,128,64]{3,1,4,2,0:T(4,128)(2,1)} %copy.86), calls=%async_computation.2 | async-start | bytes 524288 | tf_op jit(solution)/shard_map/all_to_all | solution.py:48
  164.7 9.0 %all-to-all-start.3 = ((bf16[4,4,1,128,64]{3,0,4,2,1:T(4,128)(2,1)}), bf16[4,4,1,128,64]{3,0,4,2,1:T(4,128)(2,1)S(1)}, u32[]{:S(2)}, u32[]{:S(2)}) async-start(bf16[4,4,1,128,64]{3,0,4,2,1:T(4,128)(2,1)} %copy.87), calls=%async_computation.3 | async-start | bytes 524288 | tf_op jit(solution)/shard_map/all_to_all | solution.py:48
  174.3 3.0 %copy-start.16 = (f32[2048]{0:T(1024)S(1)}, f32[2048]{0:T(1024)}, u32[]{:S(2)}) copy-start(f32[2048]{0:T(1024)} %param.22) | copy-start | bytes 24580
  185.1 41.0 %copy-start.24 = (bf16[1,2048,1024]{2,1,0:T(8,128)(2,1)S(1)}, bf16[1,2048,1024]{2,1,0:T(8,128)(2,1)}, u32[]{:S(2)}) copy-start(bf16[1,2048,1024]{2,1,0:T(8,128)(2,1)} %param.26) | copy-start | bytes 12582916
  247.4 4.9 %copy-start.23 = (f32[1,128,2]{1,2,0:T(2,128)S(1)}, f32[1,128,2]{1,2,0:T(2,128)}, u32[]{:S(2)}) copy-start(f32[1,128,2]{1,2,0:T(2,128)} %param.24) | copy-start | bytes 3076
  247.4 35.4 %all-to-all-start.5 = ((bf16[128,1,1,4,2048]{4,3,2,1,0:T(4,128)(2,1)}), bf16[128,1,1,4,2048]{4,3,2,1,0:T(4,128)(2,1)S(1)}, u32[]{:S(2)}, u32[]{:S(2)}) async-start(bf16[128,1,1,4,2048]{4,3,2,1,0:T(4,128)(2,1)} %copy.96), calls=%async_computation.5 | async-start | bytes 4194304 | tf_op jit(solution)/shard_map/all_to_all | solution.py:63
  282.8 1.3 copy-start.6
where the time goes:
time: 300 us; the launch traced here: 296 us
  local copies, waits for them, and re-layouts  69.9 us (23%)
  other arithmetic  58.2 us (19%)
  waiting for transfers between devices  55.6 us (19%)
  matrix products  42.9 us (14%)
  blocking collectives  41 us (14%)
  starting transfers between devices  27.3 us (9%)
    all_to_all x1, blocking collectives, joined_exchange(): lax.all_to_all(pieces, axis, split_axis=0, concat_axis=0, tiled=True)  41 us
    another operation x11, other arithmetic  32.9 us
    all_to_all x1, waiting for transfers between devices, joined_exchange(): lax.all_to_all(pieces, axis, split_axis=0, concat_axis=0, tiled=True)  30.4 us
    dot_general x4, matrix products, stick_head(): jnp.dot(weights, values_head[:finish], preferred_element_type=jnp.float32)  15.2 us
    another operation x5, local copies, waits for them, and re-layouts, stick_head(): suffix = lax.cumsum(breaks, axis=1, reverse=True) - breaks  15 us
    all_to_all x1, waiting for transfers between devices, sent_together(): lax.all_to_all(both, axis, split_axis=split_dim, concat_axis=concat_dim,...  14.8 us
    unnamed x63, local copies, waits for them, and re-layouts  14.8 us
    dot_general x1, matrix products, on_device(): jnp.einsum('sxcf,xfd->sxcd', inner, w_down, preferred_element_type=jnp.fl...  11.5 us
  transfers between devices with their start and end apart: 5, of which 4 were waited for; matrix products, arithmetic and copies ran while one was open for 4% of the time, Pallas kernels for 0%

commit v1 on v0

v1 whole, which is shorter than its diff:
```python
import jax
import jax.numpy as jnp
from jax import lax
from jax.sharding import PartitionSpec as P
from jax.experimental import pallas as pl
from jax.experimental.pallas import tpu as pltpu

GROUPS = 4
EXP_DEV = 1
SP = "sp"
SP_DP = ("sp", "dp")


norm_eps = 1e-05


LOG2E = 1.4426950408889634
KB = 256
QB = 256
NT = (((1,), (1,)), ((), ()))
BF16 = jnp.bfloat16
F32 = jnp.float32


def picker(rows, cols, fn):
    r = lax.broadcasted_iota(jnp.int32, (rows, cols), 0)
    c = lax.broadcasted_iota(jnp.int32, (rows, cols), 1)
    return jnp.where(fn(r, c), 1.0, 0.0).astype(BF16)


def f32dot(a, b):
    return jnp.dot(a, b, preferred_element_type=F32)


def half_pickers():
    low_low = picker(128, 128, lambda r, c: (r == c) & (c < 64))
    low_high = picker(128, 128, lambda r, c: r == c - 64)
    high_low = picker(128, 128, lambda r, c: r == c + 64)
    high_high = picker(128, 128, lambda r, c: (r == c) & (c >= 64))
    return (low_low, low_high), (high_low, high_high)


def mixer_kernel(
    q_ref, k_ref, v_ref, shift_ref, head_shift_ref, stream_ref, mix_ref, w_ref, post_ref,
    hidden_ref,
    sendbuf, recvbuf, attsend, attrecv, qs, kk, vv, off, w_vmem, normed,
    send_sem, recv_sem, asend_sem, arecv_sem, w_sem,
):
    me = lax.axis_index("sp")
    barrier = pltpu.get_barrier_semaphore()
    for d in range(1, 16):
        pl.semaphore_signal(
            barrier, inc=1, device_id={"sp": lax.rem(me + d, 16)}, device_id_type=pl.DeviceIdType.MESH
        )
    w_copy = pltpu.make_async_copy(w_ref, w_vmem, w_sem)
    w_copy.start()

    pickers = half_pickers()
    shifts = lax.dot_general(
        picker(16, 16, lambda r, c: r == c), shift_ref[...], NT, preferred_element_type=F32
    )
    for h in range(16):
        tile = slice((h // 2) * 128, (h // 2 + 1) * 128)
        first, second = pickers[h % 2]
        sendbuf[h, 0:128, :] = (f32dot(q_ref[:, tile], first) + f32dot(k_ref[:, tile], second)).astype(BF16)
        sendbuf[h, 128:192, :] = (
            f32dot(v_ref[0:64, tile], first) + f32dot(v_ref[64:128, tile], second)
        ).astype(BF16)
        sendbuf[h, 192:208, :] = jnp.broadcast_to(shifts[h:h + 1, :], (16, 128)).astype(BF16)

    pl.semaphore_wait(barrier, 15)

    def outgoing(d):
        to = lax.rem(me + d, 16)
        return pltpu.make_async_remote_copy(
            src_ref=sendbuf.at[to],
            dst_ref=recvbuf.at[me],
            send_sem=send_sem.at[d],
            recv_sem=recv_sem.at[d],
            device_id={"sp": to},
            device_id_type=pl.DeviceIdType.MESH,
        )

    for d in range(1, 16):
        outgoing(d).start()
    recvbuf[me] = sendbuf[me]
    for d in range(1, 16):
        outgoing(d).wait()

    both_low = picker(128, 128, lambda r, c: r == c % 64)
    both_high = picker(128, 128, lambda r, c: r == c % 64 + 64)
    lane = lax.broadcasted_iota(jnp.int32, (128, 128), 1)
    hs = head_shift_ref[0]
    for j in range(16):
        rows = slice(j * 128, (j + 1) * 128)
        qk = recvbuf[j, 0:128, :]
        q2 = f32dot(qk, both_low) * (LOG2E / 8.0)
        hi = q2.astype(BF16).astype(F32)
        qs[rows, :] = jnp.where(lane < 64, hi, q2 - hi).astype(BF16)
        kk[rows, :] = f32dot(qk, both_high).astype(BF16)
        vm = recvbuf[j, 128:192, :]
        vv[j * 128:j * 128 + 64, :] = f32dot(vm, both_low).astype(BF16)
        vv[j * 128 + 64:j * 128 + 128, :] = f32dot(vm, both_high).astype(BF16)
        off[0:1, rows] = (recvbuf[j, 192:208, :].astype(F32)[0:1] + hs) * LOG2E

    tri = picker(KB, KB, lambda r, c: r >= c)
    lane64 = lax.broadcasted_iota(jnp.int32, (64, 128), 1) < 64

    def reply(j):
        return pltpu.make_async_remote_copy(
            src_ref=attsend.at[j],
            dst_ref=attrecv.at[me],
            send_sem=asend_sem.at[j],
            recv_sem=arecv_sem.at[me],
            device_id={"sp": j},
            device_id_type=pl.DeviceIdType.MESH,
        )

    for qi in range(2048 // QB):
        r0 = qi * QB
        carry = jnp.zeros((QB, 1), F32)
        acc = jnp.zeros((QB, 128), F32)
        for ki in range(qi, -1, -1):
            k0 = ki * KB
            z = lax.dot_general(qs[r0:r0 + QB, :], kk[k0:k0 + KB, :], NT, preferred_element_type=F32)
            z = z + off[0:1, k0:k0 + KB]
            sp = jnp.maximum(z, jnp.log2(1.0 + jnp.exp2(jnp.minimum(z, 100.0))))
            if ki == qi:
                r = lax.broadcasted_iota(jnp.int32, (QB, KB), 0)
                c = lax.broadcasted_iota(jnp.int32, (QB, KB), 1)
                sp = jnp.where(c < r, sp, 0.0)
            hi = sp.astype(BF16)
            lo = (sp - hi.astype(F32)).astype(BF16)
            s = f32dot(hi, tri) + f32dot(lo, tri)
            w = jnp.exp2(z - (s + carry))
            if ki == qi:
                w = jnp.where(c < r, w, 0.0)
            acc = acc + f32dot(w.astype(BF16), vv[k0:k0 + KB, :])
            carry = carry + s[:, 0:1]
        for part in range(QB // 128):
            j = r0 // 128 + part
            at = part * 128
            attsend[j] = jnp.where(lane64, acc[at:at + 64], acc[at + 64:at + 128]).astype(BF16)

            @pl.when(me != j)
            def _():
                reply(j).start()

            @pl.when(me == j)
            def _():
                attrecv[j] = attsend[j]

    for j in range(16):
        @pl.when(me != j)
        def _():
            reply(j).wait_send()
            pltpu.make_async_remote_copy(
                src_ref=attsend.at[j],
                dst_ref=attrecv.at[j],
                send_sem=asend_sem.at[j],
                recv_sem=arecv_sem.at[j],
                device_id={"sp": j},
                device_id_type=pl.DeviceIdType.MESH,
            ).wait_recv()

    (low_low, low_high), (high_low, high_high) = pickers
    squares = jnp.zeros((128, 1), F32)
    tiles = []
    for p in range(8):
        even, odd = attrecv[2 * p], attrecv[2 * p + 1]
        low = f32dot(even, low_low) + f32dot(odd, low_high)
        high = f32dot(even, high_low) + f32dot(odd, high_high)
        tile = jnp.concatenate([low, high], axis=0)
        squares = squares + jnp.sum(tile * tile, axis=1, keepdims=True)
        tiles.append(tile)
    inv = lax.rsqrt(squares * (1.0 / 1024.0) + norm_eps)
    for p in range(8):
        cols = slice(p * 128, (p + 1) * 128)
        normed[:, cols] = (tiles[p] * inv * mix_ref[:, cols]).astype(BF16)
    w_copy.wait()
    totals = jnp.zeros((128, 1), F32)
    sums = []
    for n in range(8):
        cols = slice(n * 256, (n + 1) * 256)
        summed = stream_ref[:, cols].astype(F32) + f32dot(normed[...], w_vmem[:, cols])
        totals = totals + jnp.sum(summed * summed, axis=1, keepdims=True)
        sums.append(summed)
    inv = lax.rsqrt(totals * (1.0 / 2048.0) + norm_eps)
    for n in range(8):
        cols = slice(n * 256, (n + 1) * 256)
        hidden_ref[:, cols] = (sums[n] * inv * post_ref[:, cols]).astype(BF16)


def mixer(q, k, v, shift, head_shift, stream, mix_gain, out_weight, post_gain):
    vmem = pl.BlockSpec(memory_space=pltpu.VMEM)
    return pl.pallas_call(
        mixer_kernel,
        out_shape=jax.ShapeDtypeStruct((128, 2048), BF16),
        in_specs=[vmem] * 4 + [pl.BlockSpec(memory_space=pltpu.SMEM)] + [vmem] * 2
        + [pl.BlockSpec(memory_space=pl.ANY), vmem],
        out_specs=vmem,
        scratch_shapes=[
            pltpu.VMEM((16, 208, 128), BF16),
            pltpu.VMEM((16, 208, 128), BF16),
            pltpu.VMEM((16, 64, 128), BF16),
            pltpu.VMEM((16, 64, 128), BF16),
            pltpu.VMEM((2048, 128), BF16),
            pltpu.VMEM((2048, 128), BF16),
            pltpu.VMEM((2048, 128), BF16),
            pltpu.VMEM((8, 2048), F32),
            pltpu.VMEM((1024, 2048), BF16),
            pltpu.VMEM((128, 1024), BF16),
            pltpu.SemaphoreType.DMA((16,)),
            pltpu.SemaphoreType.DMA((16,)),
            pltpu.SemaphoreType.DMA((16,)),
            pltpu.SemaphoreType.DMA((16,)),
            pltpu.SemaphoreType.DMA,
        ],
        compiler_params=pltpu.CompilerParams(
            collective_id=1, has_side_effects=True, vmem_limit_bytes=56 * 2**20
        ),
    )(q, k, v, shift, head_shift, stream, mix_gain, out_weight, post_gain)


def split_up(x, dim, length):
    lengths = x.shape
    pieces = x.reshape(*lengths[:dim], length, lengths[dim] // length, *lengths[dim + 1 :])
    return jnp.moveaxis(pieces, dim, 0)


def in_order(pieces, dim):
    lengths = list(pieces.shape[1:])
    lengths[dim] *= pieces.shape[0]
    return jnp.moveaxis(pieces, 0, dim).reshape(lengths)


def joined_exchange(x, axis, axes, splits, concats):
    sizes = [lax.axis_size(a) for a in axes]
    pieces = split_up(x, splits[0], sizes[0])
    pieces = jnp.moveaxis(split_up(pieces, splits[1] + 1, sizes[1]), 0, 1)
    inside = pieces.shape[2:]
    pieces = pieces.reshape(-1, *inside)
    pieces = lax.all_to_all(pieces, axis, split_axis=0, concat_axis=0, tiled=True)
    pieces = in_order(pieces.reshape(*sizes, *inside), concats[0] + 1)
    return in_order(pieces, concats[1])


def on_device(
    stream,
    queries,
    keys_in,
    values_in,
    key_shift,
    head_shift,
    mix_gain,
    out_weight,
    post_gain,
    route,
    route_weight,
    w_gate,
    w_up,
    w_down,
):
    tokens = stream.shape[1]
    width = stream.shape[2]
    own_shift = lax.dynamic_slice_in_dim(head_shift, lax.axis_index(SP), 1)
    hidden = mixer(
        queries[0], keys_in[0], values_in[0], key_shift[0], own_shift, stream[0],
        mix_gain[None], out_weight, post_gain[None],
    )
    size_sp = lax.axis_size(SP)
    size_dp = lax.axis_size("dp")
    n_expert = EXP_DEV * size_sp * size_dp
    per_group = n_expert // GROUPS
    capacity = tokens // per_group
    expert_ids = route[0].reshape(tokens * 2)
    onehot = (expert_ids[:, None] == jnp.arange(n_expert, dtype=jnp.int32)[None, :]).astype(
        jnp.int32
    )
    ranks = jnp.sum((jnp.cumsum(onehot, axis=0) - onehot) * onehot, axis=1)
    dest = expert_ids * capacity + ranks
    rows = jnp.repeat(hidden, 2, axis=0)
    buffer = jnp.zeros((n_expert * capacity, width), jnp.bfloat16).at[dest].set(rows)
    sendable = buffer.reshape(size_sp, size_dp, EXP_DEV * capacity, width)
    received = joined_exchange(sendable, SP_DP, (SP, "dp"), (0, 1), (0, 1))
    expert_received = received.reshape(size_sp * size_dp, EXP_DEV, capacity, width)
    gate = jnp.einsum("sxcd,xdf->sxcf", expert_received, w_gate, preferred_element_type=jnp.float32)
    upper = jnp.einsum("sxcd,xdf->sxcf", expert_received, w_up, preferred_element_type=jnp.float32)
    inner = (jax.nn.silu(gate) * upper).astype(jnp.bfloat16)
    reply_result = jnp.einsum(
        "sxcf,xfd->sxcd", inner, w_down, preferred_element_type=jnp.float32
    ).astype(jnp.bfloat16)
    reply_result = reply_result.reshape(size_sp, size_dp, EXP_DEV * capacity, width)
    returned = joined_exchange(reply_result, SP_DP, (SP, "dp"), (0, 1), (0, 1))
    returned = returned.reshape(n_expert * capacity, width)
    picked = returned[dest].astype(jnp.float32).reshape(tokens, 2, width)
    moe_sum = jnp.sum(picked * route_weight[0][:, :, None], axis=1)
    result = (hidden.astype(jnp.float32) + moe_sum).astype(jnp.bfloat16)
    return result[None]


def solution(mesh):
    placed = (
        P("dp", SP, None),
        P("dp", SP, None),
        P("dp", SP, None),
        P("dp", SP, None),
        P("dp", SP, None),
        P(),
        P(),
        P(),
        P(),
        P("dp", SP, None),
        P("dp", SP, None),
        P(SP_DP, None, None),
        P(SP_DP, None, None),
        P(SP_DP, None, None),
    )
    return jax.shard_map(
        on_device, mesh=mesh, in_specs=placed, out_specs=P("dp", SP, None), check_vma=False
    )
```

time: 300 us -> 160 us (0.53); the launches traced: 296 us -> 160 us
  other arithmetic: 58.2 us -> 5.2 us
  local copies, waits for them, and re-layouts: 69.9 us -> 22.5 us
  Pallas kernels: 0 us -> 37.7 us
  matrix products: 42.9 us -> 16.7 us
  waiting for transfers between devices: 55.6 us -> 30.5 us
  starting transfers between devices: 27.3 us -> 4.55 us
    another operation x15 -> x3, other arithmetic: 42.4 us -> 0.25 us
    pallas_call x0 -> x1, Pallas kernels: none -> 37.7 us  [mixer(): pl.pallas_call(mixer_kernel, out_shape=jax.ShapeDtypeStruct((128, 2048),...]
    dot_general x9 -> x0, matrix products: 26.2 us -> none  [the longest x4 15.2 us: stick_head(): jnp.dot(weights, values_head[:finish], preferred_element_type=jnp.float32)]
    all_to_all x4 -> x0, waiting for transfers between devices: 25.2 us -> none  [the longest x1 14.8 us: sent_together(): lax.all_to_all(both, axis, split_axis=split_dim, concat_axis=concat_dim,...]
    another operation x18 -> x3, local copies, waits for them, and re-layouts: 23.5 us -> 0.02 us  [the longest x5 15 us: stick_head(): suffix = lax.cumsum(breaks, axis=1, reverse=True) - breaks]
    all_to_all x4 -> x0, starting transfers between devices: 22.4 us -> none  [the longest x1 8.59 us: on_device(): lax.all_to_all(key_shift, SP, split_axis=2, concat_axis=1, tiled=True)]
    unnamed x63 -> x11, local copies, waits for them, and re-layouts: 14.8 us -> 3.55 us
    slice x19 -> x0, local copies, waits for them, and re-layouts: 6.51 us -> none  [the longest x6 3.97 us: stick_head(): values_head[:finish]]
  transfers between devices with their start and end apart: 5 -> 1, of which waited for: 4 -> 1; matrix products, arithmetic and copies ran while one was open for 4% -> 0% of each run, Pallas kernels for 0% -> 0%
where the time goes in v1:
time: 160 us
  blocking collectives  42.5 us (27%)
  Pallas kernels  37.7 us (24%)
  waiting for transfers between devices  30.5 us (19%)
  local copies, waits for them, and re-layouts  22.5 us (14%)
  matrix products  16.7 us (10%)
  other arithmetic  5.2 us (3%)
  starting transfers between devices  4.55 us (3%)
    all_to_all x1, blocking collectives, joined_exchange(): lax.all_to_all(pieces, axis, split_axis=0, concat_axis=0, tiled=True)  42.5 us
    pallas_call x1, Pallas kernels, mixer(): pl.pallas_call(mixer_kernel, out_shape=jax.ShapeDtypeStruct((128, 2048),...  37.7 us
    all_to_all x1, waiting for transfers between devices, joined_exchange(): lax.all_to_all(pieces, axis, split_axis=0, concat_axis=0, tiled=True)  30.5 us
    dot_general x1, matrix products, on_device(): jnp.einsum('sxcf,xfd->sxcd', inner, w_down, preferred_element_type=jnp.fl...  11.5 us
    another operation x2, local copies, waits for them, and re-layouts, joined_exchange(): pieces = pieces.reshape(-1, *inside)  6.74 us
    dot_general x1, matrix products, on_device(): jnp.einsum('sxcd,xdf->sxcf', expert_received, w_up, preferred_element_typ...  5.16 us
    all_to_all x1, starting transfers between devices, joined_exchange(): lax.all_to_all(pieces, axis, split_axis=0, concat_axis=0, tiled=True)  4.55 us
    unnamed x11, local copies, waits for them, and re-layouts  3.55 us
  transfers between devices with their start and end apart: 1, of which 1 were waited for; matrix products, arithmetic and copies ran while one was open for 0% of the time, Pallas kernels for 0%

profile of v1, /device:TPU:1, one launch (start us, length us, event | category | flops | bytes accessed | tf_op | source)
XLA Modules:
  0.0 159.8 jit_solution(10924491391679363256)
XLA Ops:
  0.0 0.8 copy.29
  0.8 0.1 eq.29
  0.9 0.1 eq.25
  1.1 0.7 broadcast_multiply_fusion
  1.8 1.4 copy.27
  3.2 1.3 dynamic_slice.3.head_shift_ref
  4.5 37.7 %shard_map.136 = bf16[128,2048]{1,0:T(8,128)(2,1)} custom-call(bf16[128,1024]{1,0:T(8,128)(2,1)} %bitcast.127, bf16[128,1024]{1,0:T(8,128)(2,1)} %bitcast.128, bf16[128,1024]{1,0:T(8,128)(2,1)} %bitcast.129, bf16[128,16]{1,0:T(8,128)(2,1)} %bitcast.130, f32[1]{0:T(128)} %dynamic_slice.3.head_shift_ref, bf16[128,2048]{1,0:T(8,128)(2,1)} %bitcast.126, ...), custom_call_target="tpu_custom_call" | custom-call | tf_op jit(solution)/shard_map/pallas_call | solution.py:196
  42.2 1.7 %broadcast_in_dim.21 = bf16[128,2,2048]{2,1,0:T(2,128)(2,1)S(1)} broadcast(bf16[128,2048]{1,0:T(8,128)(2,1)} %shard_map.136), dimensions={0,2} | broadcast | bytes 1572864 | tf_op jit(solution)/shard_map/broadcast_in_dim | solution.py:282
  43.9 0.4 reshape.111
  44.3 0.1 copy.31
  44.4 0.2 fusion.37
  44.7 0.1 copy.28
  44.8 0.1 mul.38
  45.0 0.2 fusion.39
  45.2 2.8 %scatter_custom_fusion = bf16[512,2048]{1,0:T(8,128)(2,1)S(1)} fusion(s32[256]{0:T(256)S(1)} %bitcast.134, bf16[256,2048]{1,0:T(8,128)(2,1)S(1)} %reshape.111, bf16[]{:T(256)} %constant.8.clone.1), kind=kCustom, calls=%fused_computation.25 | custom fusion | bytes 2097154 | tf_op jit(solution)/shard_map/scatter | solution.py:283
  48.0 2.2 %reshape_transpose_transpose_reshape_reshape_reshape.6 = bf16[128,1,1,4,2048]{4,3,0,2,1:T(4,128)(2,1)} reshape(bf16[512,2048]{1,0:T(8,128)(2,1)S(1)} %scatter_custom_fusion) | data formatting | bytes 4194304 | tf_op jit(solution)/shard_map/reshape;transpose;transpose;reshape;reshape;reshape | solution.py:242
  50.2 0.0 copy-start.3
  50.2 42.5 %all_to_all.10 = bf16[128,1,1,4,2048]{4,3,2,1,0:T(4,128)(2,1)S(1)} all-to-all(bf16[128,1,1,4,2048]{4,3,2,1,0:T(4,128)(2,1)} %bitcast.121), channel_id=1, replica_groups=mesh['sp'=16,'dp'=8] {'sp','dp'}, dimensions={0} | all-to-all | bytes 4194304 | tf_op jit(solution)/shard_map/all_to_all | solution.py:243
  92.7 0.0 copy-done.3
  92.7 5.2 %fusion.2 = f32[128,4,1024]{2,0,1:T(8,128)} fusion(bf16[1,2048,1024]{2,1,0:T(8,128)(2,1)S(1)} %copy-done.3, bf16[16,8,1,1,4,2048]{5,4,1,0,3,2:T(4,128)(2,1)S(1)} %bitcast.122), kind=kOutput, calls=%fused_computation.4 | convolution fusion | flops 2147483648 | bytes 8388608 | tf_op jit(solution)/shard_map/sxcd,xdf->sxcf/dot_general | solution.py:288
  97.9 11.5 %fusion.9 = bf16[128,1,1,4,2048]{4,0,3,2,1:T(8,128)(2,1)} fusion(bf16[1,1024,2048]{2,1,0:T(8,128)(2,1)} %param.27, f32[128,4,1024]{2,0,1:T(8,128)} %fusion.2, bf16[1,2048,1024]{2,1,0:T(8,128)(2,1)} %param.25, bf16[16,8,1,1,4,2048]{5,4,1,0,3,2:T(4,128)(2,1)S(1)} %bitcast.123), kind=kOutput, calls=%fused_computation.9 | convolution fusion | flops 4299161600 | bytes 14680064 | tf_op jit(solution)/shard_map/sxcf,xfd->sxcd/dot_general | solution.py:290
  109.4 4.5 %copy.35 = bf16[128,1,1,4,2048]{4,3,2,1,0:T(4,128)(2,1)} copy(bf16[128,1,1,4,2048]{4,0,3,2,1:T(8,128)(2,1)} %fusion.9) | data formatting | bytes 4194304 | tf_op jit(solution)/shard_map/reshape;transpose;transpose;reshape;reshape;reshape | solution.py:242
  113.9 0.0 copy-start.2
  113.9 4.5 %all-to-all-start.1 = ((bf16[128,1,1,4,2048]{4,3,2,1,0:T(4,128)(2,1)}), bf16[128,1,1,4,2048]{4,3,2,1,0:T(4,128)(2,1)S(1)}, u32[]{:S(2)}, u32[]{:S(2)}) async-start(bf16[128,1,1,4,2048]{4,3,2,1,0:T(4,128)(2,1)} %copy.35), calls=%async_computation.1 | async-start | bytes 4194304 | tf_op jit(solution)/shard_map/all_to_all | solution.py:243
  118.5 0.0 copy-done.2
  118.5 0.1 copy.36
  118.6 30.5 %all-to-all-done.1 = bf16[128,1,1,4,2048]{4,3,2,1,0:T(4,128)(2,1)S(1)} async-done(((bf16[128,1,1,4,2048]{4,3,2,1,0:T(4,128)(2,1)}), bf16[128,1,1,4,2048]{4,3,2,1,0:T(4,128)(2,1)S(1)}, u32[]{:S(2)}, u32[]{:S(2)}) %all-to-all-start.1) | async-done | bytes 2097184 | tf_op jit(solution)/shard_map/all_to_all | solution.py:243
  149.0 0.0 copy-start
  149.1 1.3 copy-done
  150.4 2.5 %reshape_reshape.4 = bf16[512,2048]{1,0:T(8,128)(2,1)S(1)} reshape(bf16[16,8,1,4,2048]{4,3,1,0,2:T(4,128)(2,1)} %bitcast.120) | data formatting | bytes 4194304 | tf_op jit(solution)/shard_map/reshape;reshape | solution.py:295
  152.9 1.4 gather_fusion
  154.3 1.3 reshape.98
  155.7 0.0 copy-start.1
  155.7 3.2 %multiply_reduce_fusion = f32[128,2048]{1,0:T(8,128)S(1)} fusion(f32[128,2,2048]{2,1,0:T(2,128)S(1)} %reshape.98, f32[128,2]{1,0:T(8,128)S(1)} %copy.36), kind=kLoop, calls=%fused_computation.19 | loop fusion | flops 786432 | bytes 3146752 | tf_op jit(solution)/shard_map/reduce_sum | solution.py:297
  158.8 0.0 copy-done.1
  158.9 0.9 fusion.36
  (8 shorter events, 0.1 us)
Async XLA Ops:
  50.2 42.5 %copy-start.3 = (bf16[1,2048,1024]{2,1,0:T(8,128)(2,1)S(1)}, bf16[1,2048,1024]{2,1,0:T(8,128)(2,1)}, u32[]{:S(2)}) copy-start(bf16[1,2048,1024]{2,1,0:T(8,128)(2,1)} %param.26) | copy-start | bytes 12582916
  113.9 4.6 %copy-start.2 = (f32[1,128,2]{1,2,0:T(2,128)S(1)}, f32[1,128,2]{1,2,0:T(2,128)}, u32[]{:S(2)}) copy-start(f32[1,128,2]{1,2,0:T(2,128)} %param.24) | copy-start | bytes 3076
  113.9 35.1 %all-to-all-start.1 = ((bf16[128,1,1,4,2048]{4,3,2,1,0:T(4,128)(2,1)}), bf16[128,1,1,4,2048]{4,3,2,1,0:T(4,128)(2,1)S(1)}, u32[]{:S(2)}, u32[]{:S(2)}) async-start(bf16[128,1,1,4,2048]{4,3,2,1,0:T(4,128)(2,1)} %copy.35), calls=%async_computation.1 | async-start | bytes 4194304 | tf_op jit(solution)/shard_map/all_to_all | solution.py:243
  149.0 1.4 copy-start
  155.7 3.2 %copy-start.1 = (bf16[128,2048]{1,0:T(8,128)(2,1)S(1)}, bf16[128,2048]{1,0:T(8,128)(2,1)}, u32[]{:S(2)}) copy-start(bf16[128,2048]{1,0:T(8,128)(2,1)} %shard_map.136) | copy-start | bytes 1572868

commit v2 on v1

--- a/solution.py
+++ b/solution.py
@@ -5,15 +5,9 @@
 from jax.experimental import pallas as pl
 from jax.experimental.pallas import tpu as pltpu
 
-GROUPS = 4
-EXP_DEV = 1
 SP = "sp"
 SP_DP = ("sp", "dp")
-
-
 norm_eps = 1e-05
-
-
 LOG2E = 1.4426950408889634
 KB = 256
 QB = 256
@@ -222,27 +216,261 @@
     )(q, k, v, shift, head_shift, stream, mix_gain, out_weight, post_gain)
 
 
-def split_up(x, dim, length):
-    lengths = x.shape
-    pieces = x.reshape(*lengths[:dim], length, lengths[dim] // length, *lengths[dim + 1 :])
-    return jnp.moveaxis(pieces, dim, 0)
-
-
-def in_order(pieces, dim):
-    lengths = list(pieces.shape[1:])
-    lengths[dim] *= pieces.shape[0]
-    return jnp.moveaxis(pieces, 0, dim).reshape(lengths)
-
-
-def joined_exchange(x, axis, axes, splits, concats):
-    sizes = [lax.axis_size(a) for a in axes]
-    pieces = split_up(x, splits[0], sizes[0])
-    pieces = jnp.moveaxis(split_up(pieces, splits[1] + 1, sizes[1]), 0, 1)
-    inside = pieces.shape[2:]
-    pieces = pieces.reshape(-1, *inside)
-    pieces = lax.all_to_all(pieces, axis, split_axis=0, concat_axis=0, tiled=True)
-    pieces = in_order(pieces.reshape(*sizes, *inside), concats[0] + 1)
-    return in_order(pieces, concats[1])
+CHUNKS = 4
+CW = 2048 // CHUNKS
+STEP = 11
+
+
+def row_iota(rows, cols):
+    return lax.broadcasted_iota(jnp.int32, (rows, cols), 0)
+
+
+def col_iota(rows, cols):
+    return lax.broadcasted_iota(jnp.int32, (rows, cols), 1)
+
+
+def as_whole(x):
+    return x.astype(jnp.int32)
+
+
+def moe_kernel(
+    hidden_ref, route_ref, weight_ref, gate_hbm, up_hbm, down_hbm,
+    out_ref,
+    msend, mrecv, zsend, zrecv, psend, precv, osend, oret, ysend, yback,
+    gate_w, up_w, down_w, gate_acc, up_acc, inner,
+    m_ss, m_rs, z_ss, z_rs, p_ss, p_rs, o_ss, o_rs, y_ss, y_rs, w_sem,
+):
+    sp, dp = lax.axis_index("sp"), lax.axis_index("dp")
+    z, y = sp // 4, lax.rem(sp, 4)
+    place = y * 8 + dp
+
+    def on_z(at):
+        return {"sp": at * 4 + y}
+
+    def in_plane(p):
+        return {"sp": z * 4 + p // 8, "dp": lax.rem(p, 8)}
+
+    def plane_peer(i):
+        o = lax.rem(i * STEP, 32)
+        py = lax.rem(place // 8 + o // 8, 4)
+        px = lax.rem(lax.rem(place, 8) // 2 + lax.rem(o, 8) // 2, 4)
+        pc = lax.rem(place + o, 2)
+        return py * 8 + px * 2 + pc
+
+    mesh_id = pl.DeviceIdType.MESH
+    barrier = pltpu.get_barrier_semaphore()
+    for d in range(1, 4):
+        pl.semaphore_signal(barrier, inc=1, device_id=on_z(lax.rem(z + d, 4)), device_id_type=mesh_id)
+
+    def greet(i, _):
+        pl.semaphore_signal(barrier, inc=1, device_id=in_plane(plane_peer(i)), device_id_type=mesh_id)
+        return 0
+
+    lax.fori_loop(1, 32, greet, 0)
+    copies = [
+        pltpu.make_async_copy(a, b, w_sem.at[i])
+        for i, (a, b) in enumerate(((gate_hbm, gate_w), (up_hbm, up_w), (down_hbm, down_w)))
+    ]
+    for c in copies:
+        c.start()
+
+    lanes = col_iota(128, 128)
+    first, second = route_ref[:, 0:1], route_ref[:, 1:2]
+    in_first = jnp.where(lanes == first, 1.0, 0.0)
+    in_second = jnp.where(lanes == second, 1.0, 0.0)
+    before = picker(128, 128, lambda r, c: c < r)
+    named = f32dot(before, (in_first + in_second).astype(BF16))
+    rank_first = jnp.sum(in_first * named, axis=1, keepdims=True)
+    rank_second = jnp.sum(in_second * named, axis=1, keepdims=True)
+    group = lax.shift_right_logical(first, 5)
+    in_group = jnp.where(lanes == group, 1.0, 0.0)
+    within = jnp.sum(in_group * f32dot(before, in_group.astype(BF16)), axis=1, keepdims=True)
+    w0, w1 = weight_ref[:, 0:1], weight_ref[:, 1:2]
+    w0_hi, w1_hi = w0.astype(BF16).astype(F32), w1.astype(BF16).astype(F32)
+    fields = (
+        ((first & 31) + 1).astype(F32), rank_first, ((second & 31) + 1).astype(F32), rank_second,
+        w0_hi, w0 - w0_hi, w1_hi, w1 - w1_hi, group.astype(F32), within,
+    )
+    table = jnp.zeros((128, 128), F32)
+    for i, field in enumerate(fields):
+        table = jnp.where(lanes == i, field, table)
+    table = table.astype(BF16)
+    eye = picker(16, 128, lambda r, c: r == c)
+    by_lane = lax.dot_general(eye, table, NT, preferred_element_type=F32)
+    goes_to = as_whole(by_lane[8:9] * 64.0 + by_lane[9:10])
+    to_plane = jnp.where(row_iota(256, 128) == goes_to, 1.0, 0.0).astype(BF16)
+    from_plane = jnp.where(
+        col_iota(128, 256) == group * 64 + as_whole(within), 1.0, 0.0
+    ).astype(BF16)
+    msend[...] = f32dot(to_plane, table).astype(BF16).reshape(4, 64, 128)
+
+    pl.semaphore_wait(barrier, 34)
+
+    def z_copy(src, dst, ss, rs, d, c=None):
+        to = lax.rem(z + d, 4)
+        return pltpu.make_async_remote_copy(
+            src_ref=src.at[to] if c is None else src.at[c, to],
+            dst_ref=dst.at[z] if c is None else dst.at[c, z],
+            send_sem=ss.at[d] if c is None else ss.at[c, d],
+            recv_sem=rs.at[d] if c is None else rs.at[c, d],
+            device_id=on_z(to),
+            device_id_type=mesh_id,
+        )
+
+    def p_copy(src, dst, ss, rs, i, c):
+        to = plane_peer(i)
+        return pltpu.make_async_remote_copy(
+            src_ref=src.at[c, to],
+            dst_ref=dst.at[c, place],
+            send_sem=ss.at[c, i],
+            recv_sem=rs.at[c, i],
+            device_id=in_plane(to),
+            device_id_type=mesh_id,
+        )
+
+    def p_start(src, dst, ss, rs, c):
+        def one(i, _):
+            p_copy(src, dst, ss, rs, i, c).start()
+            return 0
+
+        lax.fori_loop(1, 32, one, 0)
+        dst[c, place] = src[c, place]
+
+    def p_wait(src, dst, ss, rs, c):
+        def one(i, _):
+            p_copy(src, dst, ss, rs, i, c).wait_recv()
+            return 0
+
+        lax.fori_loop(1, 32, one, 0)
+
+    for d in range(1, 4):
+        z_copy(msend, mrecv, m_ss, m_rs, d).start()
+    mrecv[z] = msend[z]
+    for c in range(CHUNKS):
+        cols = slice(c * CW, (c + 1) * CW)
+        zsend[c] = f32dot(to_plane, hidden_ref[:, cols]).astype(BF16).reshape(4, 64, CW)
+        for d in range(1, 4):
+            z_copy(zsend, zrecv, z_ss, z_rs, d, c).start()
+        zrecv[c, z] = zsend[c, z]
+
+    for d in range(1, 4):
+        z_copy(msend, mrecv, m_ss, m_rs, d).wait_recv()
+    got = mrecv[...].reshape(256, 128)
+    by_lane = lax.dot_general(eye, got, NT, preferred_element_type=F32)
+    by_row = got.astype(F32)
+
+    def slots(p, rank, source):
+        at = (as_whole(p) - 1) * 16 + source * 4 + as_whole(rank)
+        return jnp.where(p > 0.5, at, -1)
+
+    source = lax.shift_right_logical(col_iota(1, 256), 6)
+    slot0, slot1 = slots(by_lane[0:1], by_lane[1:2], source), slots(by_lane[2:3], by_lane[3:4], source)
+    at = row_iota(512, 256)
+    to_experts = jnp.where((at == slot0) | (at == slot1), 1.0, 0.0).astype(BF16)
+    source = lax.shift_right_logical(row_iota(256, 1), 6)
+    slot0 = slots(by_row[:, 0:1], by_row[:, 1:2], source)
+    slot1 = slots(by_row[:, 2:3], by_row[:, 3:4], source)
+    at = col_iota(256, 512)
+    is0, is1 = at == slot0, at == slot1
+    mix_hi = jnp.where(is0, by_row[:, 4:5], jnp.where(is1, by_row[:, 6:7], 0.0)).astype(BF16)
+    mix_lo = jnp.where(is0, by_row[:, 5:6], jnp.where(is1, by_row[:, 7:8], 0.0)).astype(BF16)
+
+    for c in range(CHUNKS):
+        for d in range(1, 4):
+            z_copy(zsend, zrecv, z_ss, z_rs, d, c).wait_recv()
+        psend[c] = f32dot(to_experts, zrecv[c].reshape(256, CW)).astype(BF16).reshape(32, 16, CW)
+        p_start(psend, precv, p_ss, p_rs, c)
+
+    for i in range(2):
+        copies[i].wait()
+    for c in range(CHUNKS):
+        p_wait(psend, precv, p_ss, p_rs, c)
+        rows = precv[c].reshape(512, CW)
+        deep = slice(c * CW, (c + 1) * CW)
+
+        def expert_in(n, _):
+            cols = pl.ds(pl.multiple_of(n * 256, 256), 256)
+            g = f32dot(rows, gate_w[deep, cols])
+            u = f32dot(rows, up_w[deep, cols])
+            if c > 0:
+                g = g + gate_acc[:, cols]
+                u = u + up_acc[:, cols]
+            if c < CHUNKS - 1:
+                gate_acc[:, cols] = g
+                up_acc[:, cols] = u
+            else:
+                inner[:, cols] = (g / (1.0 + jnp.exp(-g)) * u).astype(BF16)
+            return 0
+
+        lax.fori_loop(0, 4, expert_in, 0)
+
+    copies[2].wait()
+    for c in range(CHUNKS):
+        def expert_out(n, _):
+            cols = pl.ds(pl.multiple_of(n * 256, 256), 256)
+            o = f32dot(inner[...], down_w[:, pl.ds(pl.multiple_of(c * CW + n * 256, 256), 256)])
+            osend[c, :, :, cols] = o.astype(BF16).reshape(32, 16, 256)
+            return 0
+
+        lax.fori_loop(0, CW // 256, expert_out, 0)
+        p_start(osend, oret, o_ss, o_rs, c)
+
+    for c in range(CHUNKS):
+        p_wait(osend, oret, o_ss, o_rs, c)
+        rows = oret[c].reshape(512, CW)
+        part = f32dot(mix_hi, rows) + f32dot(mix_lo, rows)
+        ysend[c] = part.astype(BF16).reshape(4, 64, CW)
+        for d in range(1, 4):
+            z_copy(ysend, yback, y_ss, y_rs, d, c).start()
+        yback[c, z] = ysend[c, z]
+
+    for c in range(CHUNKS):
+        for d in range(1, 4):
+            z_copy(ysend, yback, y_ss, y_rs, d, c).wait_recv()
+        cols = slice(c * CW, (c + 1) * CW)
+        moe = f32dot(from_plane, yback[c].reshape(256, CW))
+        out_ref[:, cols] = (hidden_ref[:, cols].astype(F32) + moe).astype(BF16)
+
+    for d in range(1, 4):
+        z_copy(msend, mrecv, m_ss, m_rs, d).wait_send()
+        for c in range(CHUNKS):
+            z_copy(zsend, zrecv, z_ss, z_rs, d, c).wait_send()
+            z_copy(ysend, yback, y_ss, y_rs, d, c).wait_send()
+
+    def sent(i, _):
+        for c in range(CHUNKS):
+            p_copy(psend, precv, p_ss, p_rs, i, c).wait_send()
+            p_copy(osend, oret, o_ss, o_rs, i, c).wait_send()
+        return 0
+
+    lax.fori_loop(1, 32, sent, 0)
+
+
+def moe(hidden, route, route_weight, w_gate, w_up, w_down):
+    vmem = pl.BlockSpec(memory_space=pltpu.VMEM)
+    dma = pltpu.SemaphoreType.DMA
+    return pl.pallas_call(
+        moe_kernel,
+        out_shape=jax.ShapeDtypeStruct((128, 2048), BF16),
+        in_specs=[vmem] * 3 + [pl.BlockSpec(memory_space=pl.ANY)] * 3,
+        out_specs=vmem,
+        scratch_shapes=[pltpu.VMEM((4, 64, 128), BF16)] * 2
+        + [pltpu.VMEM((CHUNKS, 4, 64, CW), BF16)] * 2
+        + [pltpu.VMEM((CHUNKS, 32, 16, CW), BF16)] * 4
+        + [pltpu.VMEM((CHUNKS, 4, 64, CW), BF16)] * 2
+        + [pltpu.VMEM((2048, 1024), BF16)] * 2
+        + [pltpu.VMEM((1024, 2048), BF16)]
+        + [pltpu.VMEM((512, 1024), F32)] * 2
+        + [pltpu.VMEM((512, 1024), BF16)]
+        + [dma((4,))] * 2
+        + [dma((CHUNKS, 4))] * 2
+        + [dma((CHUNKS, 32))] * 4
+        + [dma((CHUNKS, 4))] * 2
+        + [dma((3,))],
+        compiler_params=pltpu.CompilerParams(
+            collective_id=2, has_side_effects=True, vmem_limit_bytes=58 * 2**20
+        ),
+    )(hidden, route, route_weight, w_gate, w_up, w_down)
 
 
 def on_device(
@@ -261,41 +489,12 @@
     w_up,
     w_down,
 ):
-    tokens = stream.shape[1]
-    width = stream.shape[2]
     own_shift = lax.dynamic_slice_in_dim(head_shift, lax.axis_index(SP), 1)
     hidden = mixer(
         queries[0], keys_in[0], values_in[0], key_shift[0], own_shift, stream[0],
         mix_gain[None], out_weight, post_gain[None],
     )
-    size_sp = lax.axis_size(SP)
-    size_dp = lax.axis_size("dp")
-    n_expert = EXP_DEV * size_sp * size_dp
-    per_group = n_expert // GROUPS
-    capacity = tokens // per_group
-    expert_ids = route[0].reshape(tokens * 2)
-    onehot = (expert_ids[:, None] == jnp.arange(n_expert, dtype=jnp.int32)[None, :]).astype(
-        jnp.int32
-    )
-    ranks = jnp.sum((jnp.cumsum(onehot, axis=0) - onehot) * onehot, axis=1)
-    dest = expert_ids * capacity + ranks
-    rows = jnp.repeat(hidden, 2, axis=0)
-    buffer = jnp.zeros((n_expert * capacity, width), jnp.bfloat16).at[dest].set(rows)
-    sendable = buffer.reshape(size_sp, size_dp, EXP_DEV * capacity, width)
-    received = joined_exchange(sendable, SP_DP, (SP, "dp"), (0, 1), (0, 1))
-    expert_received = received.reshape(size_sp * size_dp, EXP_DEV, capacity, width)
-    gate = jnp.einsum("sxcd,xdf->sxcf", expert_received, w_gate, preferred_element_type=jnp.float32)
-    upper = jnp.einsum("sxcd,xdf->sxcf", expert_received, w_up, preferred_element_type=jnp.float32)
-    inner = (jax.nn.silu(gate) * upper).astype(jnp.bfloat16)
-    reply_result = jnp.einsum(
-        "sxcf,xfd->sxcd", inner, w_down, preferred_element_type=jnp.float32
-    ).astype(jnp.bfloat16)
-    reply_result = reply_result.reshape(size_sp, size_dp, EXP_DEV * capacity, width)
-    returned = joined_exchange(reply_result, SP_DP, (SP, "dp"), (0, 1), (0, 1))
-    returned = returned.reshape(n_expert * capacity, width)
-    picked = returned[dest].astype(jnp.float32).reshape(tokens, 2, width)
-    moe_sum = jnp.sum(picked * route_weight[0][:, :, None], axis=1)
-    result = (hidden.astype(jnp.float32) + moe_sum).astype(jnp.bfloat16)
+    result = moe(hidden, route[0], route_weight[0], w_gate[0], w_up[0], w_down[0])
     return result[None]
 
 

time: 160 us -> 130 us (0.81)
  Pallas kernels: 37.7 us -> 122 us
  blocking collectives: 42.5 us -> 0 us
  waiting for transfers between devices: 30.5 us -> 0 us
  matrix products: 16.7 us -> 0 us
  local copies, waits for them, and re-layouts: 22.5 us -> 7.39 us
  other arithmetic: 5.2 us -> 0 us
  starting transfers between devices: 4.55 us -> 0 us
    pallas_call x0 -> x1, Pallas kernels: none -> 84.5 us  [moe(): pl.pallas_call(moe_kernel, out_shape=jax.ShapeDtypeStruct((128, 2048), BF...]
    all_to_all x1 -> x0, blocking collectives: 42.5 us -> none  [joined_exchange(): lax.all_to_all(pieces, axis, split_axis=0, concat_axis=0, tiled=True)]
    all_to_all x1 -> x0, waiting for transfers between devices: 30.5 us -> none  [joined_exchange(): lax.all_to_all(pieces, axis, split_axis=0, concat_axis=0, tiled=True)]
    dot_general x2 -> x0, matrix products: 16.7 us -> none  [the longest x1 11.5 us: on_device(): jnp.einsum('sxcf,xfd->sxcd', inner, w_down, preferred_element_type=jnp.fl...]
    another operation x6 -> x0, local copies, waits for them, and re-layouts: 9.29 us -> none  [the longest x2 6.74 us: joined_exchange(): pieces = pieces.reshape(-1, *inside)]
    all_to_all x1 -> x0, starting transfers between devices: 4.55 us -> none  [joined_exchange(): lax.all_to_all(pieces, axis, split_axis=0, concat_axis=0, tiled=True)]
    reduce_sum x2 -> x0, other arithmetic: 3.35 us -> none  [the longest x1 3.17 us: on_device(): moe_sum = jnp.sum(picked * route_weight[0][:, :, None], axis=1)]
    scatter x1 -> x0, local copies, waits for them, and re-layouts: 2.82 us -> none  [on_device(): jnp.zeros((n_expert * capacity, width), jnp.bfloat16).at[dest].set(rows)]
  transfers between devices with their start and end apart: 1 -> 0, of which waited for: 1 -> 0; matrix products, arithmetic and copies ran while one was open for 0% -> 0% of each run, Pallas kernels for 0% -> 0%
where the time goes in v2:
time: 130 us
  Pallas kernels  122 us (94%)
  local copies, waits for them, and re-layouts  7.39 us (6%)
    pallas_call x1, Pallas kernels, moe(): pl.pallas_call(moe_kernel, out_shape=jax.ShapeDtypeStruct((128, 2048), BF...  84.5 us
    pallas_call x1, Pallas kernels, mixer(): pl.pallas_call(mixer_kernel, out_shape=jax.ShapeDtypeStruct((128, 2048),...  37.6 us
    unnamed x4, local copies, waits for them, and re-layouts  6.08 us

profile of v2, /device:TPU:1, one launch (start us, length us, event | category | flops | bytes accessed | tf_op | source)
XLA Modules:
  0.0 129.6 jit_solution(2924954695614568563)
XLA Ops:
  0.0 1.3 %dynamic_slice.3.head_shift_ref = f32[1]{0:T(128)} dynamic-slice(f32[16]{0:T(128)} %param.19, s32[]{:T(128)S(6)} %select_n.3), dynamic_slice_sizes={1} | dynamic-slice | bytes 12 | tf_op jit(solution)/shard_map/dynamic_slice | solution.py:492
  1.3 1.4 %copy.15 = bf16[1,128,16]{2,1,0:T(8,128)(2,1)} copy(bf16[1,128,16]{1,2,0:T(8,128)(2,1)} %param.18) | data formatting | bytes 8192 | tf_op args[4]
  2.7 1.4 %copy.16 = s32[1,128,2]{2,1,0:T(8,128)} copy(s32[1,128,2]{1,2,0:T(2,128)} %param.23) | data formatting | bytes 2048 | tf_op args[9]
  4.1 1.4 %copy.17 = f32[1,128,2]{2,1,0:T(8,128)} copy(f32[1,128,2]{1,2,0:T(2,128)} %param.24) | data formatting | bytes 2048 | tf_op args[10]
  5.5 37.6 %shard_map.136.hidden_ref = bf16[128,2048]{1,0:T(8,128)(2,1)} custom-call(bf16[128,1024]{1,0:T(8,128)(2,1)} %bitcast.20, bf16[128,1024]{1,0:T(8,128)(2,1)} %bitcast.21, bf16[128,1024]{1,0:T(8,128)(2,1)} %bitcast.22, bf16[128,16]{1,0:T(8,128)(2,1)} %bitcast.23, f32[1]{0:T(128)} %dynamic_slice.3.head_shift_ref, bf16[128,2048]{1,0:T(8,128)(2,1)} %bitcast.17, ...), custom_call_target="tpu_custom_call" | custom-call | tf_op jit(solution)/shard_map/pallas_call | solution.py:190
  43.2 84.5 %shard_map.137 = bf16[128,2048]{1,0:T(8,128)(2,1)} custom-call(bf16[128,2048]{1,0:T(8,128)(2,1)} %shard_map.136.hidden_ref, s32[128,2]{1,0:T(8,128)} %bitcast.18, f32[128,2]{1,0:T(8,128)} %bitcast.19, bf16[2048,1024]{1,0:T(8,128)(2,1)} %bitcast.13, bf16[2048,1024]{1,0:T(8,128)(2,1)} %bitcast.14, bf16[1024,2048]{1,0:T(8,128)(2,1)} %bitcast.15), custom_call_target="tpu_custom_call" | custom-call | tf_op jit(solution)/shard_map/pallas_call | solution.py:452
  127.7 1.9 %copy.19 = bf16[1,128,2048]{2,1,0:T(8,128)(2,1)} copy(bf16[1,128,2048]{2,1,0:T(8,128)(2,1)} %bitcast.16) | data formatting | bytes 1048576

commit v3 on v1

v3 whole, which is shorter than its diff:
```python
import jax
import jax.numpy as jnp
from jax import lax
from jax.sharding import PartitionSpec as P
from jax.experimental import pallas as pl
from jax.experimental.pallas import tpu as pltpu

SP = "sp"
SP_DP = ("sp", "dp")
norm_eps = 1e-05
STEP = 11
CW = 512
OFFSETS = (1, 3, 2)
WIDE = 512

LOG2E = 1.4426950408889634
KB = 256
QB = 512
NT = (((1,), (1,)), ((), ()))
BF16 = jnp.bfloat16
F32 = jnp.float32


def picker(rows, cols, fn):
    r = lax.broadcasted_iota(jnp.int32, (rows, cols), 0)
    c = lax.broadcasted_iota(jnp.int32, (rows, cols), 1)
    return jnp.where(fn(r, c), 1.0, 0.0).astype(BF16)


def f32dot(a, b):
    return jnp.dot(a, b, preferred_element_type=F32)


def half_pickers():
    low_low = picker(128, 128, lambda r, c: (r == c) & (c < 64))
    low_high = picker(128, 128, lambda r, c: r == c - 64)
    high_low = picker(128, 128, lambda r, c: r == c + 64)
    high_high = picker(128, 128, lambda r, c: (r == c) & (c >= 64))
    return (low_low, low_high), (high_low, high_high)


def row_iota(rows, cols):
    return lax.broadcasted_iota(jnp.int32, (rows, cols), 0)


def col_iota(rows, cols):
    return lax.broadcasted_iota(jnp.int32, (rows, cols), 1)


def as_whole(x):
    return x.astype(jnp.int32)


def layer_kernel(
    q_hbm, k_hbm, v_hbm, shift_ref, head_shift_ref, stream_hbm, mix_ref, w_hbm, post_ref,
    route_ref, weight_ref, gate_hbm, up_hbm, down_hbm,
    out_ref,
    q_ref, k_ref, v_ref, stream_ref, w_vmem, hidden_ref,
    sendbuf, recvbuf, attsend, attrecv, qs, kk, vv, off, normed,
    to_plane, from_plane, to_experts, mix_hi, mix_lo, spread, gather,
    msend, mrecv, zsend, zrecv, psend, precv, osend, oret, ysend, yback,
    gate_w, up_w, down_w, xs, inner, outs,
    send_sem, recv_sem, asend_sem, arecv_sem,
    m_ss, m_rs, z_ss, z_rs, p_ss, p_rs, o_ss, o_rs, y_ss, y_rs, load_sem,
):
    me, dp = lax.axis_index("sp"), lax.axis_index("dp")
    z, y = me // 4, lax.rem(me, 4)
    place = y * 8 + dp
    mesh_id = pl.DeviceIdType.MESH

    def on_z(at):
        return {"sp": at * 4 + y}

    def in_plane(p):
        return {"sp": z * 4 + p // 8, "dp": lax.rem(p, 8)}

    def plane_peer(i):
        o = lax.rem(i * STEP, 32)
        py = lax.rem(place // 8 + o // 8, 4)
        px = lax.rem(lax.rem(place, 8) // 2 + lax.rem(o, 8) // 2, 4)
        pc = lax.rem(place + o, 2)
        return py * 8 + px * 2 + pc

    def sp_peer(d):
        return lax.rem(me + d, 16)

    barrier = pltpu.get_barrier_semaphore()

    def greet_sp(d, _):
        pl.semaphore_signal(barrier, inc=1, device_id={"sp": sp_peer(d)}, device_id_type=mesh_id)
        return 0

    def greet_plane(i, _):
        pl.semaphore_signal(barrier, inc=1, device_id=in_plane(plane_peer(i)), device_id_type=mesh_id)
        return 0

    lax.fori_loop(1, 16, greet_sp, 0)
    lax.fori_loop(1, 32, greet_plane, 0)
    loads = [
        pltpu.make_async_copy(a, b, load_sem.at[i])
        for i, (a, b) in enumerate((
            (q_hbm, q_ref), (k_hbm, k_ref), (v_hbm, v_ref), (stream_hbm, stream_ref),
            (w_hbm, w_vmem), (gate_hbm, gate_w), (up_hbm, up_w), (down_hbm, down_w),
        ))
    ]
    for c in loads:
        c.start()
    q_load, k_load, v_load, stream_load, w_load, gate_load, up_load, down_load = loads

    lanes = col_iota(128, 128)
    w_row = weight_ref[...]
    w_hi = w_row.astype(BF16).astype(F32)
    facts = jnp.concatenate(
        [route_ref[...].astype(F32), w_hi, w_row - w_hi, jnp.zeros((10, 128), F32)], axis=0
    ).astype(BF16)
    whole_eye = picker(128, 128, lambda r, c: r == c)
    by_token = lax.dot_general(whole_eye, facts, NT, preferred_element_type=F32)
    first, second = as_whole(by_token[:, 0:1]), as_whole(by_token[:, 1:2])
    in_first = jnp.where(lanes == first, 1.0, 0.0)
    in_second = jnp.where(lanes == second, 1.0, 0.0)
    before = picker(128, 128, lambda r, c: c < r)
    named = f32dot(before, (in_first + in_second).astype(BF16))
    rank_first = jnp.sum(in_first * named, axis=1, keepdims=True)
    rank_second = jnp.sum(in_second * named, axis=1, keepdims=True)
    group = (lax.shift_right_logical(first, 5) - z) & 3
    in_group = jnp.where(lanes == group, 1.0, 0.0)
    within = jnp.sum(in_group * f32dot(before, in_group.astype(BF16)), axis=1, keepdims=True)
    fields = (
        ((first & 31) + 1).astype(F32), rank_first, ((second & 31) + 1).astype(F32), rank_second,
        by_token[:, 2:3], by_token[:, 4:5], by_token[:, 3:4], by_token[:, 5:6], group.astype(F32), within,
    )
    table = jnp.zeros((128, 128), F32)
    for i, field in enumerate(fields):
        table = jnp.where(lanes == i, field, table)
    table = table.astype(BF16)
    eye = picker(16, 128, lambda r, c: r == c)
    by_lane = lax.dot_general(eye, table, NT, preferred_element_type=F32)
    goes_to = as_whole(by_lane[8:9] * 64.0 + by_lane[9:10])
    to_plane[...] = jnp.where(row_iota(256, 128) == goes_to, 1.0, 0.0).astype(BF16)
    from_plane[...] = jnp.where(
        col_iota(128, 256) == group * 64 + as_whole(within), 1.0, 0.0
    ).astype(BF16)
    msend[...] = f32dot(to_plane[...], table).astype(BF16).reshape(4, 64, 128)

    pickers = half_pickers()
    shifts = shift_ref[...].astype(F32)
    q_load.wait()
    k_load.wait()
    v_load.wait()
    for h in range(16):
        tile = slice((h // 2) * 128, (h // 2 + 1) * 128)
        first, second = pickers[h % 2]
        sendbuf[h, 0:128, :] = (f32dot(q_ref[:, tile], first) + f32dot(k_ref[:, tile], second)).astype(BF16)
        sendbuf[h, 128:192, :] = (
            f32dot(v_ref[0:64, tile], first) + f32dot(v_ref[64:128, tile], second)
        ).astype(BF16)
        sendbuf[h, 192:208, :] = jnp.broadcast_to(shifts[h:h + 1, :], (16, 128)).astype(BF16)

    pl.semaphore_wait(barrier, 46)

    def z_copy(src, dst, ss, rs, d, way=1):
        return pltpu.make_async_remote_copy(
            src_ref=src.at[d],
            dst_ref=dst.at[d],
            send_sem=ss.at[d],
            recv_sem=rs.at[d],
            device_id=on_z(lax.rem(z + 4 + way * d, 4)),
            device_id_type=mesh_id,
        )

    def p_copy(src, dst, ss, rs, i, d):
        to = plane_peer(i)
        return pltpu.make_async_remote_copy(
            src_ref=src.at[d, to],
            dst_ref=dst.at[d, place],
            send_sem=ss.at[d, i],
            recv_sem=rs.at[d, i],
            device_id=in_plane(to),
            device_id_type=mesh_id,
        )

    def p_start(src, dst, ss, rs, d):
        def one(i, _):
            p_copy(src, dst, ss, rs, i, d).start()
            return 0

        lax.fori_loop(1, 32, one, 0)
        dst[d, place] = src[d, place]

    def p_wait(src, dst, ss, rs, d):
        def one(i, _):
            p_copy(src, dst, ss, rs, i, d).wait_recv()
            return 0

        lax.fori_loop(1, 32, one, 0)

    def outgoing(d):
        to = sp_peer(d)
        return pltpu.make_async_remote_copy(
            src_ref=sendbuf.at[to],
            dst_ref=recvbuf.at[me],
            send_sem=send_sem.at[d],
            recv_sem=recv_sem.at[d],
            device_id={"sp": to},
            device_id_type=pl.DeviceIdType.MESH,
        )

    for d in range(1, 16):
        outgoing(d).start()
    recvbuf[me] = sendbuf[me]
    for d in range(1, 4):
        z_copy(msend, mrecv, m_ss, m_rs, d).start()
    mrecv[0] = msend[0]

    for d in range(1, 4):
        z_copy(msend, mrecv, m_ss, m_rs, d).wait_recv()
    def slots(p, rank, quarter):
        at = (as_whole(p) - 1) * 16 + quarter * 4 + as_whole(rank)
        return jnp.where(p > 0.5, at, -1)

    lane_quarter = lax.shift_right_logical(col_iota(1, 256), 6)
    row_quarter = lax.shift_right_logical(row_iota(256, 1), 6)
    for d in range(4):
        got = jnp.concatenate([mrecv[d]] * 4, axis=0)
        by_lane = lax.dot_general(eye, got, NT, preferred_element_type=F32)
        by_row = got.astype(F32)
        slot0 = slots(by_lane[0:1], by_lane[1:2], lane_quarter)
        slot1 = slots(by_lane[2:3], by_lane[3:4], lane_quarter)
        at = row_iota(512, 256)
        to_experts[d] = jnp.where((at == slot0) | (at == slot1), 1.0, 0.0).astype(BF16)
        slot0 = slots(by_row[:, 0:1], by_row[:, 1:2], row_quarter)
        slot1 = slots(by_row[:, 2:3], by_row[:, 3:4], row_quarter)
        at = col_iota(256, 512)
        is0, is1 = at == slot0, at == slot1
        mix_hi[d] = jnp.where(is0, by_row[:, 4:5], jnp.where(is1, by_row[:, 6:7], 0.0)).astype(BF16)
        mix_lo[d] = jnp.where(is0, by_row[:, 5:6], jnp.where(is1, by_row[:, 7:8], 0.0)).astype(BF16)

    def message_row(stacked):
        return (stacked & 127) // 4 * 16 + lax.shift_right_logical(stacked, 7) * 4 + (stacked & 3)

    spread[...] = jnp.where(row_iota(512, 512) == message_row(col_iota(1, 512)), 1.0, 0.0).astype(BF16)
    gather[...] = jnp.where(col_iota(512, 512) == message_row(row_iota(512, 1)), 1.0, 0.0).astype(BF16)

    for d in range(1, 16):
        outgoing(d).wait()

    both_low = picker(128, 128, lambda r, c: r == c % 64)
    both_high = picker(128, 128, lambda r, c: r == c % 64 + 64)
    lane = lax.broadcasted_iota(jnp.int32, (128, 128), 1)
    hs = head_shift_ref[me]
    for j in range(16):
        rows = slice(j * 128, (j + 1) * 128)
        qk = recvbuf[j, 0:128, :]
        q2 = f32dot(qk, both_low) * (LOG2E / 8.0)
        hi = q2.astype(BF16).astype(F32)
        qs[rows, :] = jnp.where(lane < 64, hi, q2 - hi).astype(BF16)
        kk[rows, :] = f32dot(qk, both_high).astype(BF16)
        vm = recvbuf[j, 128:192, :]
        vv[j * 128:j * 128 + 64, :] = f32dot(vm, both_low).astype(BF16)
        vv[j * 128 + 64:j * 128 + 128, :] = f32dot(vm, both_high).astype(BF16)
        off[0:1, rows] = (recvbuf[j, 192:208, :].astype(F32)[0:1] + hs) * LOG2E

    tri = picker(KB, KB, lambda r, c: r >= c)
    lane64 = lax.broadcasted_iota(jnp.int32, (64, 128), 1) < 64

    def reply(j):
        return pltpu.make_async_remote_copy(
            src_ref=attsend.at[j],
            dst_ref=attrecv.at[me],
            send_sem=asend_sem.at[j],
            recv_sem=arecv_sem.at[me],
            device_id={"sp": j},
            device_id_type=pl.DeviceIdType.MESH,
        )

    for qi in range(2048 // QB):
        r0 = qi * QB
        carry = jnp.zeros((QB, 1), F32)
        acc = jnp.zeros((QB, 128), F32)
        for ki in range((r0 + QB) // KB - 1, -1, -1):
            k0 = ki * KB
            logit = lax.dot_general(qs[r0:r0 + QB, :], kk[k0:k0 + KB, :], NT, preferred_element_type=F32)
            logit = logit + off[0:1, k0:k0 + KB]
            sp = jnp.maximum(logit, jnp.log2(1.0 + jnp.exp2(jnp.minimum(logit, 100.0))))
            masked = k0 >= r0
            if masked:
                r = lax.broadcasted_iota(jnp.int32, (QB, KB), 0)
                c = lax.broadcasted_iota(jnp.int32, (QB, KB), 1)
                earlier = c - r < r0 - k0
                sp = jnp.where(earlier, sp, 0.0)
            hi = sp.astype(BF16)
            lo = (sp - hi.astype(F32)).astype(BF16)
            s = f32dot(hi, tri) + f32dot(lo, tri)
            w = jnp.exp2((logit - s) - carry)
            if masked:
                w = jnp.where(earlier, w, 0.0)
            acc = acc + f32dot(w.astype(BF16), vv[k0:k0 + KB, :])
            carry = carry + s[:, 0:1]
        for part in range(QB // 128):
            j = r0 // 128 + part
            at = part * 128
            attsend[j] = jnp.where(lane64, acc[at:at + 64], acc[at + 64:at + 128]).astype(BF16)

            @pl.when(me != j)
            def _():
                reply(j).start()

            @pl.when(me == j)
            def _():
                attrecv[j] = attsend[j]

    for j in range(16):
        @pl.when(me != j)
        def _():
            reply(j).wait_send()
            pltpu.make_async_remote_copy(
                src_ref=attsend.at[j],
                dst_ref=attrecv.at[j],
                send_sem=asend_sem.at[j],
                recv_sem=arecv_sem.at[j],
                device_id={"sp": j},
                device_id_type=pl.DeviceIdType.MESH,
            ).wait_recv()

    (low_low, low_high), (high_low, high_high) = pickers
    squares = jnp.zeros((128, 1), F32)
    tiles = []
    for p in range(8):
        even, odd = attrecv[2 * p], attrecv[2 * p + 1]
        low = f32dot(even, low_low) + f32dot(odd, low_high)
        high = f32dot(even, high_low) + f32dot(odd, high_high)
        tile = jnp.concatenate([low, high], axis=0)
        squares = squares + jnp.sum(tile * tile, axis=1, keepdims=True)
        tiles.append(tile)
    inv = lax.rsqrt(squares * (1.0 / 1024.0) + norm_eps)
    for p in range(8):
        cols = slice(p * 128, (p + 1) * 128)
        normed[:, cols] = (tiles[p] * inv * mix_ref[:, cols]).astype(BF16)
    w_load.wait()
    stream_load.wait()
    totals = jnp.zeros((128, 1), F32)
    sums = []
    for n in range(8):
        cols = slice(n * 256, (n + 1) * 256)
        summed = stream_ref[:, cols].astype(F32) + f32dot(normed[...], w_vmem[:, cols])
        totals = totals + jnp.sum(summed * summed, axis=1, keepdims=True)
        sums.append(summed)
    inv = lax.rsqrt(totals * (1.0 / 2048.0) + norm_eps)
    for n in range(8):
        cols = slice(n * 256, (n + 1) * 256)
        hidden_ref[:, cols] = (sums[n] * inv * post_ref[:, cols]).astype(BF16)

    for q in range(4):
        rows = f32dot(to_plane[...], hidden_ref[:, q * CW:(q + 1) * CW]).astype(BF16)
        for d in range(4):
            zsend[d, q] = rows[d * 64:(d + 1) * 64]
    for d in OFFSETS:
        z_copy(zsend, zrecv, z_ss, z_rs, d).start()

    def dispatch(d, source):
        if d:
            z_copy(zsend, zrecv, z_ss, z_rs, d).wait_recv()
        psend[d] = f32dot(to_experts[d], source[d].reshape(256, CW)).astype(BF16).reshape(32, 16, CW)
        p_start(psend, precv, p_ss, p_rs, d)

    def expert(d):
        p_wait(psend, precv, p_ss, p_rs, d)
        stacked = f32dot(gather[...], precv[d].reshape(512, CW)).astype(BF16)
        for q in range(4):
            xs[:, q * CW:(q + 1) * CW] = stacked[q * 128:(q + 1) * 128]

        def first_half(n, _):
            cols = pl.ds(pl.multiple_of(n * WIDE, WIDE), WIDE)
            g = f32dot(xs[...], gate_w[:, cols])
            u = f32dot(xs[...], up_w[:, cols])
            inner[:, cols] = (g / (1.0 + jnp.exp(-g)) * u).astype(BF16)
            return 0

        lax.fori_loop(0, 1024 // WIDE, first_half, 0)

        def second_half(q, _):
            cols = pl.ds(pl.multiple_of(q * CW, CW), CW)
            outs[q] = f32dot(inner[...], down_w[:, cols]).astype(BF16)
            return 0

        lax.fori_loop(0, 4, second_half, 0)
        osend[d] = f32dot(spread[...], outs[...].reshape(512, CW)).astype(BF16).reshape(32, 16, CW)

    def combine(d):
        p_wait(osend, oret, o_ss, o_rs, d)
        rows = oret[d].reshape(512, CW)
        part = f32dot(mix_hi[d], rows) + f32dot(mix_lo[d], rows)
        if d:
            ysend[d] = part.astype(BF16).reshape(4, 64, CW)
            z_copy(ysend, yback, y_ss, y_rs, d, -1).start()
        else:
            yback[0] = part.astype(BF16).reshape(4, 64, CW)

    dispatch(0, zsend)
    dispatch(1, zrecv)
    dispatch(3, zrecv)
    gate_load.wait()
    up_load.wait()
    down_load.wait()
    expert(0)
    dispatch(2, zrecv)
    for d in OFFSETS:
        expert(d)
        p_start(osend, oret, o_ss, o_rs, d)
    p_start(osend, oret, o_ss, o_rs, 0)
    for d in OFFSETS:
        combine(d)
    combine(0)
    for d in OFFSETS:
        z_copy(ysend, yback, y_ss, y_rs, d, -1).wait_recv()
    for q in range(4):
        cols = slice(q * CW, (q + 1) * CW)
        moe = f32dot(from_plane[...], jnp.concatenate([yback[d, q] for d in range(4)], axis=0))
        out_ref[:, cols] = (hidden_ref[:, cols].astype(F32) + moe).astype(BF16)

    for d in range(1, 4):
        z_copy(msend, mrecv, m_ss, m_rs, d).wait_send()
        z_copy(zsend, zrecv, z_ss, z_rs, d).wait_send()
        z_copy(ysend, yback, y_ss, y_rs, d, -1).wait_send()

    def sent(i, _):
        for d in range(4):
            p_copy(psend, precv, p_ss, p_rs, i, d).wait_send()
            p_copy(osend, oret, o_ss, o_rs, i, d).wait_send()
        return 0

    lax.fori_loop(1, 32, sent, 0)


def layer(*arrays):
    vmem = pl.BlockSpec(memory_space=pltpu.VMEM)
    smem = pl.BlockSpec(memory_space=pltpu.SMEM)
    hbm = pl.BlockSpec(memory_space=pltpu.HBM)
    dma = pltpu.SemaphoreType.DMA
    return pl.pallas_call(
        layer_kernel,
        out_shape=jax.ShapeDtypeStruct((128, 2048), BF16),
        in_specs=[hbm] * 3 + [vmem, smem, hbm, vmem, hbm, vmem, vmem, vmem] + [hbm] * 3,
        out_specs=vmem,
        scratch_shapes=[pltpu.VMEM((128, 1024), BF16)] * 3
        + [pltpu.VMEM((128, 2048), BF16), pltpu.VMEM((1024, 2048), BF16), pltpu.VMEM((128, 2048), BF16)]
        + [pltpu.VMEM((16, 208, 128), BF16)] * 2
        + [pltpu.VMEM((16, 64, 128), BF16)] * 2
        + [pltpu.VMEM((2048, 128), BF16)] * 3
        + [pltpu.VMEM((8, 2048), F32), pltpu.VMEM((128, 1024), BF16)]
        + [pltpu.VMEM((256, 128), BF16), pltpu.VMEM((128, 256), BF16), pltpu.VMEM((4, 512, 256), BF16)]
        + [pltpu.VMEM((4, 256, 512), BF16)] * 2
        + [pltpu.VMEM((512, 512), BF16)] * 2
        + [pltpu.VMEM((4, 64, 128), BF16)] * 2
        + [pltpu.VMEM((4, 4, 64, CW), BF16)] * 2
        + [pltpu.VMEM((4, 32, 16, CW), BF16)] * 4
        + [pltpu.VMEM((4, 4, 64, CW), BF16)] * 2
        + [pltpu.VMEM((2048, 1024), BF16)] * 2
        + [pltpu.VMEM((1024, 2048), BF16)]
        + [pltpu.VMEM((128, 2048), BF16), pltpu.VMEM((128, 1024), BF16), pltpu.VMEM((4, 128, CW), BF16)]
        + [dma((16,))] * 4
        + [dma((4,))] * 2
        + [dma((4,))] * 2
        + [dma((4, 32))] * 4
        + [dma((4,))] * 2
        + [dma((8,))],
        compiler_params=pltpu.CompilerParams(
            collective_id=1, has_side_effects=True, vmem_limit_bytes=60 * 2**20
        ),
    )(*arrays)


def on_device(
    stream,
    queries,
    keys_in,
    values_in,
    key_shift,
    head_shift,
    mix_gain,
    out_weight,
    post_gain,
    route,
    route_weight,
    w_gate,
    w_up,
    w_down,
):
    result = layer(
        queries[0], keys_in[0], values_in[0], key_shift[0].T, head_shift, stream[0], mix_gain[None],
        out_weight, post_gain[None], route[0].T, route_weight[0].T, w_gate[0], w_up[0], w_down[0],
    )
    return result[None]


def solution(mesh):
    placed = (
        P("dp", SP, None),
        P("dp", SP, None),
        P("dp", SP, None),
        P("dp", SP, None),
        P("dp", SP, None),
        P(),
        P(),
        P(),
        P(),
        P("dp", SP, None),
        P("dp", SP, None),
        P(SP_DP, None, None),
        P(SP_DP, None, None),
        P(SP_DP, None, None),
    )
    return jax.shard_map(
        on_device, mesh=mesh, in_specs=placed, out_specs=P("dp", SP, None), check_vma=False
    )
```

time: 160 us -> 106 us (0.66)
  Pallas kernels: 37.7 us -> 104 us
  blocking collectives: 42.5 us -> 0 us
  waiting for transfers between devices: 30.5 us -> 0 us
  local copies, waits for them, and re-layouts: 22.5 us -> 1.88 us
  matrix products: 16.7 us -> 0 us
  other arithmetic: 5.2 us -> 0 us
  starting transfers between devices: 4.55 us -> 0 us
    pallas_call x1, Pallas kernels: 37.7 us -> 104 us  [layer(): pl.pallas_call(layer_kernel, out_shape=jax.ShapeDtypeStruct((128, 2048),...]
    all_to_all x1 -> x0, blocking collectives: 42.5 us -> none  [joined_exchange(): lax.all_to_all(pieces, axis, split_axis=0, concat_axis=0, tiled=True)]
    all_to_all x1 -> x0, waiting for transfers between devices: 30.5 us -> none  [joined_exchange(): lax.all_to_all(pieces, axis, split_axis=0, concat_axis=0, tiled=True)]
    dot_general x2 -> x0, matrix products: 16.7 us -> none  [the longest x1 11.5 us: on_device(): jnp.einsum('sxcf,xfd->sxcd', inner, w_down, preferred_element_type=jnp.fl...]
    another operation x6 -> x0, local copies, waits for them, and re-layouts: 9.29 us -> none  [the longest x2 6.74 us: joined_exchange(): pieces = pieces.reshape(-1, *inside)]
    all_to_all x1 -> x0, starting transfers between devices: 4.55 us -> none  [joined_exchange(): lax.all_to_all(pieces, axis, split_axis=0, concat_axis=0, tiled=True)]
    reduce_sum x2 -> x0, other arithmetic: 3.35 us -> none  [the longest x1 3.17 us: on_device(): moe_sum = jnp.sum(picked * route_weight[0][:, :, None], axis=1)]
    scatter x1 -> x0, local copies, waits for them, and re-layouts: 2.82 us -> none  [on_device(): jnp.zeros((n_expert * capacity, width), jnp.bfloat16).at[dest].set(rows)]
  transfers between devices with their start and end apart: 1 -> 0, of which waited for: 1 -> 0; matrix products, arithmetic and copies ran while one was open for 0% -> 0% of each run, Pallas kernels for 0% -> 0%
where the time goes in v3:
time: 106 us
  Pallas kernels  104 us (98%)
  local copies, waits for them, and re-layouts  1.88 us (2%)
    pallas_call x1, Pallas kernels, layer(): pl.pallas_call(layer_kernel, out_shape=jax.ShapeDtypeStruct((128, 2048),...  104 us

profile of v3, /device:TPU:1, one launch (start us, length us, event | category | flops | bytes accessed | tf_op | source)
XLA Modules:
  0.0 106.2 jit_solution(16146641978349207298)
XLA Ops:
  0.0 104.3 %shard_map.136 = bf16[128,2048]{1,0:T(8,128)(2,1)} custom-call(bf16[128,1024]{1,0:T(8,128)(2,1)} %bitcast.24, bf16[128,1024]{1,0:T(8,128)(2,1)} %bitcast.25, bf16[128,1024]{1,0:T(8,128)(2,1)} %bitcast.26, bf16[16,128]{1,0:T(8,128)(2,1)} %bitcast.28, f32[16]{0:T(128)} %head_shift_ref.1, bf16[128,2048]{1,0:T(8,128)(2,1)} %bitcast.23, f32[1,1024]{1,0:T(1,128)} %bitcast.29, ...), custom_call_target="tpu_custom_call" | custom-call | tf_op jit(solution)/shard_map/pallas_call | solution.py:440
  104.3 1.9 %copy.16 = bf16[1,128,2048]{2,1,0:T(8,128)(2,1)} copy(bf16[1,128,2048]{2,1,0:T(8,128)(2,1)} %bitcast.22) | data formatting | bytes 1048576

commit v4 on v3

--- a/solution.py
+++ b/solution.py
@@ -11,6 +11,10 @@
 STEP = 11
 CW = 512
 OFFSETS = (1, 3, 2)
+ROUTES = (
+    (1, 1), (3, 3), (1, 3), (3, 1), (0, 1), (1, 0), (0, 3), (3, 0),
+    (0, 2), (2, 0), (2, 2), (1, 2), (2, 1), (3, 2), (2, 3),
+)
 WIDE = 512
 
 LOG2E = 1.4426950408889634
@@ -81,13 +85,19 @@
         pc = lax.rem(place + o, 2)
         return py * 8 + px * 2 + pc
 
-    def sp_peer(d):
-        return lax.rem(me + d, 16)
+    turn = 1 - 2 * lax.rem(dp, 2)
+
+    def sp_peer(i, way):
+        dz, dy = ROUTES[i]
+        to_z = lax.rem(z + 4 + way * turn * dz, 4)
+        return to_z * 4 + lax.rem(y + 4 + way * turn * dy, 4)
 
     barrier = pltpu.get_barrier_semaphore()
 
     def greet_sp(d, _):
-        pl.semaphore_signal(barrier, inc=1, device_id={"sp": sp_peer(d)}, device_id_type=mesh_id)
+        pl.semaphore_signal(
+            barrier, inc=1, device_id={"sp": lax.rem(me + d, 16)}, device_id_type=mesh_id
+        )
         return 0
 
     def greet_plane(i, _):
@@ -106,6 +116,73 @@
     for c in loads:
         c.start()
     q_load, k_load, v_load, stream_load, w_load, gate_load, up_load, down_load = loads
+
+    pickers = half_pickers()
+    shifts = shift_ref[...].astype(F32)
+    q_load.wait()
+    k_load.wait()
+    v_load.wait()
+    for h in range(16):
+        tile = slice((h // 2) * 128, (h // 2 + 1) * 128)
+        first, second = pickers[h % 2]
+        sendbuf[h, 0:128, :] = (f32dot(q_ref[:, tile], first) + f32dot(k_ref[:, tile], second)).astype(BF16)
+        sendbuf[h, 128:192, :] = (
+            f32dot(v_ref[0:64, tile], first) + f32dot(v_ref[64:128, tile], second)
+        ).astype(BF16)
+        sendbuf[h, 192:208, :] = jnp.broadcast_to(shifts[h:h + 1, :], (16, 128)).astype(BF16)
+
+    pl.semaphore_wait(barrier, 46)
+
+    def z_copy(src, dst, ss, rs, d, way=1):
+        return pltpu.make_async_remote_copy(
+            src_ref=src.at[d],
+            dst_ref=dst.at[d],
+            send_sem=ss.at[d],
+            recv_sem=rs.at[d],
+            device_id=on_z(lax.rem(z + 4 + way * d, 4)),
+            device_id_type=mesh_id,
+        )
+
+    def p_copy(src, dst, ss, rs, i, d):
+        to = plane_peer(i)
+        return pltpu.make_async_remote_copy(
+            src_ref=src.at[d, to],
+            dst_ref=dst.at[d, place],
+            send_sem=ss.at[d, i],
+            recv_sem=rs.at[d, i],
+            device_id=in_plane(to),
+            device_id_type=mesh_id,
+        )
+
+    def p_start(src, dst, ss, rs, d):
+        def one(i, _):
+            p_copy(src, dst, ss, rs, i, d).start()
+            return 0
+
+        lax.fori_loop(1, 32, one, 0)
+        dst[d, place] = src[d, place]
+
+    def p_wait(src, dst, ss, rs, d):
+        def one(i, _):
+            p_copy(src, dst, ss, rs, i, d).wait_recv()
+            return 0
+
+        lax.fori_loop(1, 32, one, 0)
+
+    def outgoing(i):
+        to = sp_peer(i, 1)
+        return pltpu.make_async_remote_copy(
+            src_ref=sendbuf.at[to],
+            dst_ref=recvbuf.at[me],
+            send_sem=send_sem.at[i],
+            recv_sem=recv_sem.at[i],
+            device_id={"sp": to},
+            device_id_type=mesh_id,
+        )
+
+    for i in range(15):
+        outgoing(i).start()
+    recvbuf[me] = sendbuf[me]
 
     lanes = col_iota(128, 128)
     w_row = weight_ref[...]
@@ -142,72 +219,6 @@
     ).astype(BF16)
     msend[...] = f32dot(to_plane[...], table).astype(BF16).reshape(4, 64, 128)
 
-    pickers = half_pickers()
-    shifts = shift_ref[...].astype(F32)
-    q_load.wait()
-    k_load.wait()
-    v_load.wait()
-    for h in range(16):
-        tile = slice((h // 2) * 128, (h // 2 + 1) * 128)
-        first, second = pickers[h % 2]
-        sendbuf[h, 0:128, :] = (f32dot(q_ref[:, tile], first) + f32dot(k_ref[:, tile], second)).astype(BF16)
-        sendbuf[h, 128:192, :] = (
-            f32dot(v_ref[0:64, tile], first) + f32dot(v_ref[64:128, tile], second)
-        ).astype(BF16)
-        sendbuf[h, 192:208, :] = jnp.broadcast_to(shifts[h:h + 1, :], (16, 128)).astype(BF16)
-
-    pl.semaphore_wait(barrier, 46)
-
-    def z_copy(src, dst, ss, rs, d, way=1):
-        return pltpu.make_async_remote_copy(
-            src_ref=src.at[d],
-            dst_ref=dst.at[d],
-            send_sem=ss.at[d],
-            recv_sem=rs.at[d],
-            device_id=on_z(lax.rem(z + 4 + way * d, 4)),
-            device_id_type=mesh_id,
-        )
-
-    def p_copy(src, dst, ss, rs, i, d):
-        to = plane_peer(i)
-        return pltpu.make_async_remote_copy(
-            src_ref=src.at[d, to],
-            dst_ref=dst.at[d, place],
-            send_sem=ss.at[d, i],
-            recv_sem=rs.at[d, i],
-            device_id=in_plane(to),
-            device_id_type=mesh_id,
-        )
-
-    def p_start(src, dst, ss, rs, d):
-        def one(i, _):
-            p_copy(src, dst, ss, rs, i, d).start()
-            return 0
-
-        lax.fori_loop(1, 32, one, 0)
-        dst[d, place] = src[d, place]
-
-    def p_wait(src, dst, ss, rs, d):
-        def one(i, _):
-            p_copy(src, dst, ss, rs, i, d).wait_recv()
-            return 0
-
-        lax.fori_loop(1, 32, one, 0)
-
-    def outgoing(d):
-        to = sp_peer(d)
-        return pltpu.make_async_remote_copy(
-            src_ref=sendbuf.at[to],
-            dst_ref=recvbuf.at[me],
-            send_sem=send_sem.at[d],
-            recv_sem=recv_sem.at[d],
-            device_id={"sp": to},
-            device_id_type=pl.DeviceIdType.MESH,
-        )
-
-    for d in range(1, 16):
-        outgoing(d).start()
-    recvbuf[me] = sendbuf[me]
     for d in range(1, 4):
         z_copy(msend, mrecv, m_ss, m_rs, d).start()
     mrecv[0] = msend[0]
@@ -241,24 +252,28 @@
     spread[...] = jnp.where(row_iota(512, 512) == message_row(col_iota(1, 512)), 1.0, 0.0).astype(BF16)
     gather[...] = jnp.where(col_iota(512, 512) == message_row(row_iota(512, 1)), 1.0, 0.0).astype(BF16)
 
-    for d in range(1, 16):
-        outgoing(d).wait()
-
     both_low = picker(128, 128, lambda r, c: r == c % 64)
     both_high = picker(128, 128, lambda r, c: r == c % 64 + 64)
-    lane = lax.broadcasted_iota(jnp.int32, (128, 128), 1)
+    lane = col_iota(128, 128)
     hs = head_shift_ref[me]
-    for j in range(16):
-        rows = slice(j * 128, (j + 1) * 128)
+
+    def unpack(j):
+        at = pl.multiple_of(j * 128, 128)
+        rows = pl.ds(at, 128)
         qk = recvbuf[j, 0:128, :]
         q2 = f32dot(qk, both_low) * (LOG2E / 8.0)
         hi = q2.astype(BF16).astype(F32)
         qs[rows, :] = jnp.where(lane < 64, hi, q2 - hi).astype(BF16)
         kk[rows, :] = f32dot(qk, both_high).astype(BF16)
         vm = recvbuf[j, 128:192, :]
-        vv[j * 128:j * 128 + 64, :] = f32dot(vm, both_low).astype(BF16)
-        vv[j * 128 + 64:j * 128 + 128, :] = f32dot(vm, both_high).astype(BF16)
+        vv[pl.ds(at, 64), :] = f32dot(vm, both_low).astype(BF16)
+        vv[pl.ds(pl.multiple_of(at + 64, 64), 64), :] = f32dot(vm, both_high).astype(BF16)
         off[0:1, rows] = (recvbuf[j, 192:208, :].astype(F32)[0:1] + hs) * LOG2E
+
+    unpack(me)
+    for i in range(15):
+        outgoing(i).wait_recv()
+        unpack(sp_peer(i, -1))
 
     tri = picker(KB, KB, lambda r, c: r >= c)
     lane64 = lax.broadcasted_iota(jnp.int32, (64, 128), 1) < 64
@@ -418,6 +433,8 @@
         moe = f32dot(from_plane[...], jnp.concatenate([yback[d, q] for d in range(4)], axis=0))
         out_ref[:, cols] = (hidden_ref[:, cols].astype(F32) + moe).astype(BF16)
 
+    for i in range(15):
+        outgoing(i).wait_send()
     for d in range(1, 4):
         z_copy(msend, mrecv, m_ss, m_rs, d).wait_send()
         z_copy(zsend, zrecv, z_ss, z_rs, d).wait_send()
@@ -439,7 +456,7 @@
     dma = pltpu.SemaphoreType.DMA
     return pl.pallas_call(
         layer_kernel,
-        out_shape=jax.ShapeDtypeStruct((128, 2048), BF16),
+        out_shape=pltpu.VMEM((128, 2048), BF16),
         in_specs=[hbm] * 3 + [vmem, smem, hbm, vmem, hbm, vmem, vmem, vmem] + [hbm] * 3,
         out_specs=vmem,
         scratch_shapes=[pltpu.VMEM((128, 1024), BF16)] * 3

time: 106 us -> 104 us (0.981); the launches traced: 106 us -> 103 us
  Pallas kernels: 104 us -> 102 us
  local copies, waits for them, and re-layouts: 1.88 us -> 0.8 us
    pallas_call x1, Pallas kernels: 104 us -> 102 us  [layer(): pl.pallas_call(layer_kernel, out_shape=pltpu.VMEM((128, 2048), BF16), in_...]
    unnamed x1, local copies, waits for them, and re-layouts: 1.88 us -> 0.8 us
where the time goes in v4:
time: 104 us; the launch traced here: 103 us
  Pallas kernels  102 us (98%)
    pallas_call x1, Pallas kernels, layer(): pl.pallas_call(layer_kernel, out_shape=pltpu.VMEM((128, 2048), BF16), in_...  102 us

profile of v4, /device:TPU:1, one launch (start us, length us, event | category | flops | bytes accessed | tf_op | source)
XLA Modules:
  0.0 102.9 jit_solution(9661774177478184020)
XLA Ops:
  0.0 102.1 %shard_map.136 = bf16[128,2048]{1,0:T(8,128)(2,1)S(1)} custom-call(bf16[128,1024]{1,0:T(8,128)(2,1)} %bitcast.24, bf16[128,1024]{1,0:T(8,128)(2,1)} %bitcast.25, bf16[128,1024]{1,0:T(8,128)(2,1)} %bitcast.26, bf16[16,128]{1,0:T(8,128)(2,1)} %bitcast.28, f32[16]{0:T(128)} %head_shift_ref.1, bf16[128,2048]{1,0:T(8,128)(2,1)} %bitcast.23, f32[1,1024]{1,0:T(1,128)} %bitcast.29, ...), custom_call_target="tpu_custom_call" | custom-call | tf_op jit(solution)/shard_map/pallas_call | solution.py:457
  102.1 0.8 copy.16

commit v5 on v4

--- a/solution.py
+++ b/solution.py
@@ -8,7 +8,11 @@
 SP = "sp"
 SP_DP = ("sp", "dp")
 norm_eps = 1e-05
-STEP = 11
+TURNS = (
+    ((1, 1), (3, 3)), ((1, 3), (3, 1)), ((0, 1), (1, 0), (0, 3), (3, 0)),
+    ((0, 2), (2, 0)), ((2, 2),), ((1, 2), (2, 1), (3, 2), (2, 3)),
+)
+PLANE = tuple(dy * 8 + dx * 2 + dc for turn in TURNS for dc in (0, 1) for dy, dx in turn) + (1,)
 CW = 512
 OFFSETS = (1, 3, 2)
 ROUTES = (
@@ -78,10 +82,9 @@
     def in_plane(p):
         return {"sp": z * 4 + p // 8, "dp": lax.rem(p, 8)}
 
-    def plane_peer(i):
-        o = lax.rem(i * STEP, 32)
+    def plane_peer(o):
         py = lax.rem(place // 8 + o // 8, 4)
-        px = lax.rem(lax.rem(place, 8) // 2 + lax.rem(o, 8) // 2, 4)
+        px = lax.rem(lax.rem(place, 8) // 2 + o % 8 // 2, 4)
         pc = lax.rem(place + o, 2)
         return py * 8 + px * 2 + pc
 
@@ -155,11 +158,8 @@
         )
 
     def p_start(src, dst, ss, rs, d):
-        def one(i, _):
-            p_copy(src, dst, ss, rs, i, d).start()
-            return 0
-
-        lax.fori_loop(1, 32, one, 0)
+        for o in PLANE:
+            p_copy(src, dst, ss, rs, o, d).start()
         dst[d, place] = src[d, place]
 
     def p_wait(src, dst, ss, rs, d):

time: 104 us -> 99.7 us (0.959)
  Pallas kernels: 102 us -> 98.7 us
    pallas_call x1, Pallas kernels: 102 us -> 98.7 us  [layer(): pl.pallas_call(layer_kernel, out_shape=pltpu.VMEM((128, 2048), BF16), in_...]
where the time goes in v5:
time: 99.7 us; the launch traced here: 99.5 us
  Pallas kernels  98.7 us (99%)
    pallas_call x1, Pallas kernels, layer(): pl.pallas_call(layer_kernel, out_shape=pltpu.VMEM((128, 2048), BF16), in_...  98.7 us

profile of v5, /device:TPU:1, one launch (start us, length us, event | category | flops | bytes accessed | tf_op | source)
XLA Modules:
  0.0 99.5 jit_solution(7949535188884366750)
XLA Ops:
  0.0 98.7 %shard_map.136 = bf16[128,2048]{1,0:T(8,128)(2,1)S(1)} custom-call(bf16[128,1024]{1,0:T(8,128)(2,1)} %bitcast.24, bf16[128,1024]{1,0:T(8,128)(2,1)} %bitcast.25, bf16[128,1024]{1,0:T(8,128)(2,1)} %bitcast.26, bf16[16,128]{1,0:T(8,128)(2,1)} %bitcast.28, f32[16]{0:T(128)} %head_shift_ref.1, bf16[128,2048]{1,0:T(8,128)(2,1)} %bitcast.23, f32[1,1024]{1,0:T(1,128)} %bitcast.29, ...), custom_call_target="tpu_custom_call" | custom-call | tf_op jit(solution)/shard_map/pallas_call | solution.py:457
  98.8 0.8 copy.16
